TPU v7x, 256 devices: a 8x8x2 block of a 8x8x16 slice. The times are simulated.
256 devices in a mesh: grp: 2 (over z), ep: 64 (over y, x), tp: 2 (over core).
Axes of the slice: x: 8, y: 8, z: 2, core: 2. Of those that a mesh axis runs over, the one named last changes fastest.
The devices are a block of a 8x8x16 slice.
Arguments:
- tokens: bfloat16 [4096, 2048], P(('grp', 'ep')), parts along dimension 0, may hold values from -6 to 6
- in_gain: bfloat16 [2048], replicated, may hold values from 0.099609375 to 1.8984375
- route_expert: int32 [4096, 6], P(('grp', 'ep')), parts along dimension 0, may hold values from 0 to 63, all different within a row; in each aligned block of 32 rows (0 to 31, 32 to 63, ...) at most 4 rows name the same one
- route_weight: float32 [4096, 6], P(('grp', 'ep')), parts along dimension 0, may hold values from 0.05 to 1
- gate_weight: bfloat16 [64, 2048, 768], P('ep', None, 'tp'), may hold values from -0.125 to 0.125
- up_weight: bfloat16 [64, 2048, 768], P('ep', None, 'tp'), may hold values from -0.125 to 0.125
- down_weight: bfloat16 [64, 768, 2048], P('ep', 'tp'), may hold values from -1 to 1
- shared_gate: bfloat16 [2048, 768], P(None, 'tp'), may hold values from -0.125 to 0.125
- shared_up: bfloat16 [2048, 768], P(None, 'tp'), may hold values from -0.125 to 0.125
- shared_down: bfloat16 [768, 2048], P('tp'), may hold values from -1 to 1
- out_gain: bfloat16 [2048], P('tp'), may hold values from 0.099609375 to 1.8984375
Outputs:
- mixed: bfloat16 [4096, 2048], P(('grp', 'ep'), 'tp'), parts along dimension 0
There are 2 independent parts, one for each index of `grp`. A program takes and returns all parts, laid end to end along the dimension named above; an argument that names none is the same for every part. Nothing has to cross between parts.
Inputs may be any that keep to these rules, and one draw needn't show every extreme that they name: `route_expert`: each row names 6 different experts. Among the rows of one device no expert is named more than 4 times, a bound that some block reaches.
All inputs are finite; a program needn't handle non-finite values.
Results may differ from a plain program's by a relative error of at most 0.0077.
Values may be sent and summed in bfloat16 or wider, within the bound.
No kernel may reach another device: no remote copies, remote signals or barrier semaphores. Data moves between devices by JAX's collectives and lax.ppermute only.
A program may use at most 64 MiB of HBM per device.

v0:
```python
import jax
import jax.numpy as jnp
from jax import lax
from jax.sharding import PartitionSpec as P

EPSILON = 1e-06


def laid_out(blocks, dim):
    shape = list(blocks.shape[1:])
    shape[dim] *= blocks.shape[0]
    return jnp.moveaxis(blocks, 0, dim).reshape(shape)


def from_everyone(array, axis):
    devices = lax.axis_size(axis)
    return lax.all_to_all(
        jnp.broadcast_to(array[None], (devices, *array.shape)), axis, 0, 0, tiled=True
    )


def collect(array, axis, dim):
    return laid_out(from_everyone(array, axis), dim)


def in_blocks(array, dim, devices):
    before, after = (array.shape[:dim], array.shape[dim + 1 :])
    return jnp.moveaxis(array.reshape(*before, devices, -1, *after), dim, 0)


def sent_and_summed(array, axis, dim):
    devices = lax.axis_size(axis)
    blocks = lax.all_to_all(in_blocks(array, dim, devices), axis, 0, 0, tiled=True)
    return jnp.sum(blocks.astype(jnp.float32), axis=0)


def gathered_total(array, axis):
    return lax.all_gather(array, axis).sum(0)


def normalize(values, gain_vector):
    floats = values.astype(jnp.float32)
    scaled = floats * lax.rsqrt(jnp.mean(floats * floats, axis=-1, keepdims=True) + EPSILON)
    return (scaled * gain_vector.astype(jnp.float32)).astype(jnp.bfloat16)


def swiglu_hidden(inputs, gate_here, up_here):
    gate_value = jnp.dot(inputs, gate_here, preferred_element_type=jnp.float32)
    upward = jnp.dot(inputs, up_here, preferred_element_type=jnp.float32)
    return (jax.nn.silu(gate_value) * upward).astype(jnp.bfloat16)


def slot_tables(routes_here, experts, capacity):
    picked_count = routes_here.shape[0] * routes_here.shape[1]
    flattened = routes_here.reshape(picked_count)
    onehot = (flattened[:, None] == jnp.arange(experts, dtype=jnp.int32)[None, :]).astype(jnp.int32)
    earlier = jnp.cumsum(onehot, axis=0) - onehot
    ranked = jnp.sum(earlier * onehot, axis=1)
    slot_index = flattened * capacity + ranked
    source_token = jnp.arange(picked_count, dtype=jnp.int32) // routes_here.shape[1]
    matches = slot_index[None, :] == jnp.arange(experts * capacity, dtype=jnp.int32)[:, None]
    filled = jnp.any(matches, axis=1)
    slot_owner = jnp.sum(jnp.where(matches, source_token[None, :], 0), axis=1)
    return (slot_index, filled, slot_owner)


def body(
    tokens,
    in_gain,
    route_expert,
    route_weight,
    gate_weight,
    up_weight,
    down_weight,
    shared_gate,
    shared_up,
    shared_down,
    out_gain,
):
    experts = lax.axis_size("ep")
    local_tokens, model_width = tokens.shape
    top_count = route_expert.shape[1]
    capacity = max(2, (local_tokens * top_count * 4 + 3 * experts - 1) // (3 * experts))
    normed = normalize(tokens, in_gain)
    slot_index, filled, slot_owner = slot_tables(route_expert, experts, capacity)
    outgoing = jnp.where(filled[:, None], normed[slot_owner], jnp.zeros((), jnp.bfloat16))
    outgoing = outgoing.reshape(experts, capacity, model_width)
    half_width = model_width // lax.axis_size("tp")
    own_half = lax.dynamic_slice_in_dim(outgoing, lax.axis_index("tp") * half_width, half_width, 2)
    arrived = lax.all_to_all(own_half, "ep", split_axis=0, concat_axis=0, tiled=True)
    arrived = collect(arrived, "tp", 2)
    expert_rows = arrived.reshape(experts * capacity, model_width)
    expert_part = jnp.dot(
        swiglu_hidden(expert_rows, gate_weight[0], up_weight[0]),
        down_weight[0],
        preferred_element_type=jnp.float32,
    )
    shared_part = jnp.dot(
        swiglu_hidden(normed, shared_gate, shared_up),
        shared_down,
        preferred_element_type=jnp.float32,
    )
    summed = sent_and_summed(
        jnp.concatenate([expert_part, shared_part], axis=0).astype(jnp.bfloat16), "tp", 1
    )
    rounded = summed.astype(jnp.bfloat16)
    result_rows = rounded[: experts * capacity].reshape(experts, capacity, rounded.shape[1])
    shared_rows = rounded[experts * capacity :].astype(jnp.float32)
    returned = lax.all_to_all(result_rows, "ep", split_axis=0, concat_axis=0, tiled=True)
    returned = returned.reshape(experts * capacity, rounded.shape[1])
    picked = (
        returned[slot_index].astype(jnp.float32)
        * route_weight.reshape(local_tokens * top_count)[:, None]
    )
    combined = shared_rows + jnp.sum(
        picked.reshape(local_tokens, top_count, rounded.shape[1]), axis=1
    )
    squares = gathered_total(jnp.sum(combined * combined, axis=1), "tp")
    scaled = combined * lax.rsqrt(squares / model_width + EPSILON)[:, None]
    return (scaled * out_gain.astype(jnp.float32)).astype(jnp.bfloat16)


def solution(mesh):
    return jax.shard_map(
        body,
        mesh=mesh,
        in_specs=(
            P(("grp", "ep"), None),
            P(),
            P(("grp", "ep"), None),
            P(("grp", "ep"), None),
            P("ep", None, "tp"),
            P("ep", None, "tp"),
            P("ep", "tp", None),
            P(None, "tp"),
            P(None, "tp"),
            P("tp", None),
            P("tp"),
        ),
        out_specs=P(("grp", "ep"), "tp"),
        check_vma=False,
    )
```

profile of v0, /device:TPU:513, one launch (start us, length us, event | category | flops | bytes accessed | tf_op | source)
XLA Modules:
  0.0 102.2 jit_solution(11588395061193541111)
XLA Ops:
  0.0 0.9 copy.29
  3.0 1.0 %fusion.21 = f32[32]{0:T(128)S(1)} fusion(bf16[32,2048]{1,0:T(8,128)(2,1)} %param.11), kind=kLoop, calls=%fused_computation.23 | loop fusion | flops 196576 | bytes 131200 | tf_op jit(solution)/shard_map/reduce_sum | solution.py:43
  4.0 1.0 fusion.23
  5.0 1.4 %gather_fusion = bf16[256,2048]{1,0:T(8,128)(2,1)S(1)} fusion(bf16[32,2048]{1,0:T(8,128)(2,1)S(1)} %fusion.23, s32[1024]{0:T(1024)S(1)} %pad_clamp_fusion.1), kind=kCustom, calls=%fused_computation | custom fusion | bytes 2098176 | tf_op jit(solution)/shard_map/gather | solution.py:86
  6.4 1.2 %gather.9 = bf16[64,4,2048]{2,1,0:T(4,128)(2,1)} reshape(bf16[256,2048]{1,0:T(8,128)(2,1)S(1)} %gather_fusion) | data formatting | bytes 2097152 | tf_op jit(solution)/shard_map/gather | solution.py:86
  7.8 2.2 %dynamic-slice_select_fusion = bf16[64,4,1024]{2,1,0:T(4,128)(2,1)} fusion(bf16[64,4,2048]{2,1,0:T(4,128)(2,1)} %gather.9, s32[]{:T(128)S(6)} %select_n.45, pred[64,4]{1,0:T(8,128)(4,1)S(1)} %broadcast_in_dim.28), kind=kLoop, calls=%fused_computation.15 | loop fusion | flops 262144 | bytes 1048836 | tf_op jit(solution)/shard_map/jit(_where)/select_n | solution.py:86
  9.9 21.8 %all-to-all-start = ((bf16[64,4,1024]{2,1,0:T(4,128)(2,1)}), bf16[64,4,1024]{2,1,0:T(4,128)(2,1)S(1)}, u32[]{:S(2)}, u32[]{:S(2)}) async-start(bf16[64,4,1024]{2,1,0:T(4,128)(2,1)} %dynamic-slice_select_fusion), calls=%async_computation | async-start | bytes 1048576 | tf_op jit(solution)/shard_map/all_to_all | solution.py:90
  31.7 2.6 %copy.37 = bf16[2048,384]{1,0:T(8,128)(2,1)} copy(bf16[2048,384]{0,1:T(8,128)(2,1)} %bitcast.61) | data formatting | bytes 3145728 | tf_op jit(solution)/shard_map/dot_general | solution.py:93
  34.4 1.7 %fusion.36 = f32[32,384]{1,0:T(8,128)S(1)} fusion(bf16[32,2048]{1,0:T(8,128)(2,1)S(1)} %fusion.23, bf16[2048,384]{1,0:T(8,128)(2,1)} %param.18), kind=kOutput, calls=%fused_computation.64 | convolution fusion | flops 50331648 | bytes 1753088 | tf_op jit(solution)/shard_map/dot_general | solution.py:48
  36.1 2.6 %convolution_convert_fusion = bf16[32,2048]{1,0:T(8,128)(2,1)S(1)} fusion(bf16[384,2048]{1,0:T(8,128)(2,1)} %param.20, bf16[32,2048]{1,0:T(8,128)(2,1)S(1)} %fusion.23, bf16[2048,384]{1,0:T(8,128)(2,1)} %param.19, f32[32,384]{1,0:T(8,128)S(1)} %fusion.36), kind=kOutput, calls=%fused_computation.2 | convolution fusion | flops 100802560 | bytes 3457024 | tf_op jit(solution)/shard_map/dot_general | solution.py:98
  38.8 6.2 %all-to-all-done = bf16[64,4,1024]{2,1,0:T(4,128)(2,1)S(1)} async-done(((bf16[64,4,1024]{2,1,0:T(4,128)(2,1)}), bf16[64,4,1024]{2,1,0:T(4,128)(2,1)S(1)}, u32[]{:S(2)}, u32[]{:S(2)}) %all-to-all-start) | async-done | bytes 524320 | tf_op jit(solution)/shard_map/all_to_all | solution.py:90
  45.2 10.5 %all_to_all.20 = bf16[2,64,4,1024]{3,2,1,0:T(4,128)(2,1)S(1)} all-to-all(bf16[2,64,4,1024]{3,2,1,0:T(4,128)(2,1)S(1)} %broadcast_in_dim.48), channel_id=1, replica_groups=mesh['grp'=2,'ep'=64,'tp'=2] {'tp'}, dimensions={0} | all-to-all | bytes 2097152 | tf_op jit(solution)/shard_map/all_to_all | solution.py:17
  55.7 1.1 %copy.32 = bf16[64,4,2,1024]{3,2,1,0:T(2,128)(2,1)S(1)} copy(bf16[64,4,2,1024]{3,1,0,2:T(4,128)(2,1)S(1)} %bitcast.59) | data formatting | bytes 2097152 | tf_op jit(solution)/shard_map/transpose | solution.py:12
  57.1 1.1 %copy-done.1 = bf16[1,2048,384]{2,1,0:T(8,128)(2,1)S(1)} copy-done((bf16[1,2048,384]{2,1,0:T(8,128)(2,1)S(1)}, bf16[1,2048,384]{2,1,0:T(8,128)(2,1)}, u32[]{:S(2)}) %copy-start.1) | copy-done | bytes 1572888
  58.9 3.7 %convolution_convert_fusion.1 = bf16[256,2,1024]{2,0,1:T(8,128)(2,1)} fusion(bf16[2,1024,384]{2,1,0:T(8,128)(2,1)} %bitcast.62, bf16[256,2048]{1,0:T(8,128)(2,1)S(1)} %bitcast.58, bf16[1,2048,384]{2,1,0:T(8,128)(2,1)S(1)} %copy-done, f32[256,384]{1,0:T(8,128)S(1)} %fusion.2), kind=kOutput, calls=%fused_computation.7 | convolution fusion | flops 806420480 | bytes 5636096 | tf_op jit(solution)/shard_map/dot_general | solution.py:93
  62.6 1.3 %maximum_bitcast_fusion = bf16[2,288,1024]{2,1,0:T(8,128)(2,1)S(1)} fusion(bf16[32,2,1024]{2,0,1:T(8,128)(2,1)S(1)} %bitcast.63, bf16[256,2,1024]{2,0,1:T(8,128)(2,1)} %convolution_convert_fusion.1), kind=kLoop, calls=%fused_computation.9 | loop fusion | flops 2359296 | bytes 2359296 | tf_op jit(solution)/shard_map/transpose | solution.py:28
  64.0 4.7 %all_to_all.21 = bf16[2,288,1024]{2,1,0:T(8,128)(2,1)S(1)} all-to-all(bf16[2,288,1024]{2,1,0:T(8,128)(2,1)S(1)} %maximum_bitcast_fusion), channel_id=1, replica_groups=mesh['grp'=2,'ep'=64,'tp'=2] {'tp'}, dimensions={0} | all-to-all | bytes 2359296 | tf_op jit(solution)/shard_map/all_to_all | solution.py:33
  69.0 1.0 reshape.125
  70.0 6.5 %all-to-all-start.3 = ((bf16[64,4,1024]{2,1,0:T(4,128)(2,1)}), bf16[64,4,1024]{2,1,0:T(4,128)(2,1)S(1)}, u32[]{:S(2)}, u32[]{:S(2)}) async-start(bf16[64,4,1024]{2,1,0:T(4,128)(2,1)} %reshape.125), calls=%async_computation.3 | async-start | bytes 1048576 | tf_op jit(solution)/shard_map/all_to_all | solution.py:109
  78.1 14.7 %all-to-all-done.3 = bf16[64,4,1024]{2,1,0:T(4,128)(2,1)S(1)} async-done(((bf16[64,4,1024]{2,1,0:T(4,128)(2,1)}), bf16[64,4,1024]{2,1,0:T(4,128)(2,1)S(1)}, u32[]{:S(2)}, u32[]{:S(2)}) %all-to-all-start.3) | async-done | bytes 524320 | tf_op jit(solution)/shard_map/all_to_all | solution.py:109
  93.0 1.8 %gather_fusion.1 = bf16[192,1024]{1,0:T(8,128)(2,1)} fusion(bf16[256,1024]{1,0:T(8,128)(2,1)S(1)} %reshape.126, s32[1024]{0:T(1024)S(1)} %pad_clamp_fusion), kind=kCustom, calls=%fused_computation.1 | custom fusion | bytes 787200 | tf_op jit(solution)/shard_map/gather | solution.py:112
  94.7 1.1 %reshape.128 = f32[32,6,1024]{2,1,0:T(8,128)S(1)} reshape(bf16[192,1024]{1,0:T(8,128)(2,1)} %gather_fusion.1) | data formatting | bytes 1179648 | tf_op jit(solution)/shard_map/convert_element_type | solution.py:112
  96.6 4.8 %all-reduce.1 = f32[64]{0:T(128)S(1)} all-reduce(f32[64]{0:T(128)S(1)} %dynamic-update-slice), channel_id=2, replica_groups=mesh['grp'=2,'ep'=64,'tp'=2] {'tp'}, use_global_device_ids=true, to_apply=%add.1 | all-reduce | flops 64 | bytes 512
  101.5 0.7 multiply_convert_fusion
  (50 shorter events, 5.7 us)
Async XLA Ops:
  0.0 58.9 %copy-start = (bf16[1,2048,384]{2,1,0:T(8,128)(2,1)S(1)}, bf16[1,2048,384]{2,1,0:T(8,128)(2,1)}, u32[]{:S(2)}) copy-start(bf16[1,2048,384]{2,1,0:T(8,128)(2,1)} %param.16) | copy-start | bytes 4718596
  9.9 35.0 %all-to-all-start = ((bf16[64,4,1024]{2,1,0:T(4,128)(2,1)}), bf16[64,4,1024]{2,1,0:T(4,128)(2,1)S(1)}, u32[]{:S(2)}, u32[]{:S(2)}) async-start(bf16[64,4,1024]{2,1,0:T(4,128)(2,1)} %dynamic-slice_select_fusion), calls=%async_computation | async-start | bytes 1048576 | tf_op jit(solution)/shard_map/all_to_all | solution.py:90
  56.8 1.4 %copy-start.1 = (bf16[1,2048,384]{2,1,0:T(8,128)(2,1)S(1)}, bf16[1,2048,384]{2,1,0:T(8,128)(2,1)}, u32[]{:S(2)}) copy-start(bf16[1,2048,384]{2,1,0:T(8,128)(2,1)} %param.15) | copy-start | bytes 4718596
  68.9 7.6 %copy-start.2 = (s32[32,6]{0,1:T(8,128)S(1)}, s32[32,6]{0,1:T(8,128)}, u32[]{:S(2)}) copy-start(s32[32,6]{0,1:T(8,128)} %param.13) | copy-start | bytes 2308
  69.0 7.8 %copy-start.3 = (f32[32,6]{0,1:T(8,128)S(1)}, f32[32,6]{0,1:T(8,128)}, u32[]{:S(2)}) copy-start(f32[32,6]{0,1:T(8,128)} %param.14) | copy-start | bytes 2308
  69.0 7.9 %copy-start.4 = (bf16[1024]{0:T(1024)(128)(2,1)S(1)}, bf16[1024]{0:T(1024)(128)(2,1)}, u32[]{:S(2)}) copy-start(bf16[1024]{0:T(1024)(128)(2,1)} %param.21) | copy-start | bytes 6148
  69.0 7.9 %copy-start.5 = (u32[256]{0:T(256)S(1)}, u32[256]{0:T(256)}, u32[]{:S(2)}) copy-start(u32[256]{0:T(256)} %constant.63) | copy-start | bytes 3076
  70.0 22.8 %all-to-all-start.3 = ((bf16[64,4,1024]{2,1,0:T(4,128)(2,1)}), bf16[64,4,1024]{2,1,0:T(4,128)(2,1)S(1)}, u32[]{:S(2)}, u32[]{:S(2)}) async-start(bf16[64,4,1024]{2,1,0:T(4,128)(2,1)} %reshape.125), calls=%async_computation.3 | async-start | bytes 1048576 | tf_op jit(solution)/shard_map/all_to_all | solution.py:109
where the time goes:
time: 103 us; the launch traced here: 102 us
  starting transfers between devices  28.3 us (27%)
  waiting for transfers between devices  20.9 us (20%)
  blocking collectives  20 us (19%)
  local copies, waits for them, and re-layouts  14.5 us (14%)
  other arithmetic  8.86 us (9%)
  matrix products  8.8 us (9%)
    all_to_all x1, starting transfers between devices, body(): lax.all_to_all(own_half, 'ep', split_axis=0, concat_axis=0, tiled=True)  21.8 us
    all_to_all x1, waiting for transfers between devices, body(): lax.all_to_all(result_rows, 'ep', split_axis=0, concat_axis=0, tiled=True)  14.7 us
    all_to_all x1, blocking collectives, from_everyone(): lax.all_to_all(jnp.broadcast_to(array[None], (devices, *array.shape)), ax...  10.5 us
    all_to_all x1, starting transfers between devices, body(): lax.all_to_all(result_rows, 'ep', split_axis=0, concat_axis=0, tiled=True)  6.49 us
    all_to_all x1, waiting for transfers between devices, body(): lax.all_to_all(own_half, 'ep', split_axis=0, concat_axis=0, tiled=True)  6.16 us
    unnamed x1, blocking collectives  4.82 us
    all_to_all x1, blocking collectives, sent_and_summed(): lax.all_to_all(in_blocks(array, dim, devices), axis, 0, 0, tiled=True)  4.7 us
    dot_general x1, matrix products, body(): jnp.dot(swiglu_hidden(expert_rows, gate_weight[0], up_weight[0]), down_we...  3.71 us
  transfers between devices with their start and end apart: 2, of which 2 were waited for; matrix products, arithmetic and copies ran while one was open for 8% of the time, Pallas kernels for 0%

commit v1 on v0

v1 whole, which is shorter than its diff:
```python
import functools

import jax
import jax.numpy as jnp
from jax import lax
from jax.experimental import pallas as pl
from jax.experimental.pallas import tpu as pltpu
from jax.sharding import PartitionSpec as P

EPSILON = 1e-06
F32 = jnp.float32
BF16 = jnp.bfloat16
VMEM = pltpu.VMEM


def whole():
    return pl.BlockSpec(memory_space=VMEM)


def iota(shape, dim):
    return lax.broadcasted_iota(jnp.int32, shape, dim)


def chosen(route, core, slots, pieces, experts, values=None):
    top, tokens = route.shape
    rows, lanes = experts * slots * pieces, pieces * tokens
    row, lane = iota((rows, lanes), 0), iota((rows, lanes), 1)
    expert = row // (slots * pieces)
    tiled = jnp.concatenate([route] * pieces, axis=1)
    hits = [tiled[k : k + 1] == expert for k in range(top)]
    named = functools.reduce(jnp.logical_or, hits)
    before, after = iota((lanes, lanes), 0), iota((lanes, lanes), 1)
    earlier = (before // tokens == after // tokens) & (before < after)
    ones = jnp.where(named, 1.0, 0.0).astype(BF16)
    rank = jnp.dot(ones, jnp.where(earlier, 1.0, 0.0).astype(BF16), preferred_element_type=F32)
    wanted = ((row // pieces) % slots + slots * core).astype(F32)
    keep = named & (rank == wanted) & (lane // tokens == row % pieces)
    if values is None:
        return jnp.where(keep, 1.0, 0.0)
    spread = jnp.concatenate([values] * pieces, axis=1)
    total = jnp.zeros((rows, lanes), F32)
    for k in range(top):
        total = jnp.where(hits[k], spread[k : k + 1], total)
    return jnp.where(keep, total, 0.0)


def dispatch_kernel(tokens_ref, gain_ref, route_ref, send_ref, normed_ref, *, slots, pieces, experts):
    core = lax.axis_index("tp")
    values = tokens_ref[...].astype(F32)
    scaled = values * lax.rsqrt(jnp.mean(values * values, axis=-1, keepdims=True) + EPSILON)
    normed = (scaled * gain_ref[...].astype(F32)).astype(BF16)
    normed_ref[...] = normed
    piece = normed.shape[1] // pieces
    stacked = jnp.concatenate([normed[:, q * piece : (q + 1) * piece] for q in range(pieces)], axis=0)
    pick = chosen(route_ref[...], core, slots, pieces, experts).astype(BF16)
    send_ref[...] = jnp.dot(pick, stacked, preferred_element_type=F32).astype(BF16)


def shared_kernel(
    normed_ref, gate_ref, up_ref, down_ref, route_ref, weight_ref, part_ref, mix_ref, *, slots, pieces, experts
):
    core = lax.axis_index("tp")
    normed = normed_ref[...]
    gate = jnp.dot(normed, gate_ref[...], preferred_element_type=F32)
    upward = jnp.dot(normed, up_ref[...], preferred_element_type=F32)
    hidden = (gate * jax.nn.sigmoid(gate) * upward).astype(BF16)
    tokens, piece = normed.shape[0], normed.shape[1] // pieces
    for q in range(pieces):
        part_ref[q * tokens : (q + 1) * tokens, :] = jnp.dot(
            hidden, down_ref[:, q * piece : (q + 1) * piece], preferred_element_type=F32
        )
    mix = chosen(route_ref[...], core, slots, pieces, experts, weight_ref[...]).T
    high = mix.astype(BF16)
    mix_ref[: mix.shape[0], :] = high
    mix_ref[mix.shape[0] :, :] = (mix - high.astype(F32)).astype(BF16)


def gathering(half, pieces):
    to, frm = iota((half * pieces, half * pieces), 0), iota((half * pieces, half * pieces), 1)
    return jnp.where(frm == (to % half) * pieces + to // half, 1.0, 0.0).astype(BF16)


def expert_kernel(
    rows_ref, gate_ref, up_ref, down_ref, gate2_ref, up2_ref, down2_ref, out_ref, *, pieces
):
    total = rows_ref.shape[0]
    rows, block = total // pieces, total // 2
    half = rows // 2
    piece = rows_ref.shape[1]
    order = gathering(half, pieces)
    parts = [
        jnp.dot(order, rows_ref[h * block : (h + 1) * block, :], preferred_element_type=F32).astype(BF16)
        for h in range(2)
    ]
    inputs = jnp.concatenate(
        [
            jnp.concatenate([parts[h][q * half : (q + 1) * half] for h in range(2)], axis=0)
            for q in range(pieces)
        ],
        axis=1,
    )
    hidden = []
    for g, u in ((gate_ref, up_ref), (gate2_ref, up2_ref)):
        gate = jnp.dot(inputs, g[...], preferred_element_type=F32)
        upward = jnp.dot(inputs, u[...], preferred_element_type=F32)
        hidden.append((gate * jax.nn.sigmoid(gate) * upward).astype(BF16))
    back = order.T
    results = []
    for q in range(pieces):
        span = slice(q * piece, (q + 1) * piece)
        results.append(
            (
                jnp.dot(hidden[0], down_ref[:, span], preferred_element_type=F32)
                + jnp.dot(hidden[1], down2_ref[:, span], preferred_element_type=F32)
            ).astype(BF16)
        )
    for h in range(2):
        lined = jnp.concatenate([r[h * half : (h + 1) * half] for r in results], axis=0)
        out_ref[h * block : (h + 1) * block, :] = jnp.dot(back, lined, preferred_element_type=F32).astype(BF16)


def combine_kernel(mix_ref, returned_ref, part_ref, out_ref):
    both = jnp.dot(mix_ref[...], returned_ref[...], preferred_element_type=F32)
    size = both.shape[0] // 2
    out_ref[...] = part_ref[...] + both[:size] + both[size:]


def closing_kernel(mine_ref, other_ref, gain_ref, out_ref, total_ref, *, pieces):
    core = lax.axis_index("tp")
    total = mine_ref[...] + other_ref[...]
    total_ref[...] = total
    tokens, piece = total.shape[0] // pieces, total.shape[1]
    squares = jnp.sum(total * total, axis=1, keepdims=True)
    squares = functools.reduce(jnp.add, [squares[q * tokens : (q + 1) * tokens] for q in range(pieces)])
    scale = lax.rsqrt(squares / (pieces * piece) + EPSILON)
    mine = out_ref.shape[1] // piece
    gain = gain_ref[...].astype(F32)
    for q in range(mine):
        start = pl.multiple_of((core * mine + q) * tokens, 8)
        values = total_ref[pl.ds(start, tokens), :] * scale
        out_ref[:, q * piece : (q + 1) * piece] = (values * gain[:, q * piece : (q + 1) * piece]).astype(BF16)


def body(
    tokens,
    in_gain,
    route_expert,
    route_weight,
    gate_weight,
    up_weight,
    down_weight,
    shared_gate,
    shared_up,
    shared_down,
    out_gain,
):
    experts, cores = lax.axis_size("ep"), lax.axis_size("tp")
    local_tokens, width = tokens.shape
    top_count = route_expert.shape[1]
    capacity = max(2, (local_tokens * top_count * 4 + 3 * experts - 1) // (3 * experts))
    slots = capacity // cores
    pieces = 8 // slots
    piece = width // pieces
    rows = experts * slots * pieces
    sizes = dict(slots=slots, pieces=pieces, experts=experts)
    params = pltpu.CompilerParams(vmem_limit_bytes=48 * 1024 * 1024)

    swap = [(i, (i + 1) % cores) for i in range(cores)]
    weights = (gate_weight[0], up_weight[0], down_weight[0])
    others = tuple(lax.ppermute(w, "tp", swap) for w in weights)

    send, normed = pl.pallas_call(
        functools.partial(dispatch_kernel, **sizes),
        out_shape=(
            jax.ShapeDtypeStruct((rows, piece), BF16),
            jax.ShapeDtypeStruct((local_tokens, width), BF16),
        ),
        in_specs=[whole()] * 3,
        out_specs=(whole(), whole()),
        name="dispatch",
    )(tokens, in_gain.reshape(1, width), route_expert.T)
    with jax.named_scope("outward"):
        arrived = lax.all_to_all(send.reshape(experts, slots * pieces, piece), "ep", 0, 0, tiled=True)

    part, mix = pl.pallas_call(
        functools.partial(shared_kernel, **sizes),
        out_shape=(
            jax.ShapeDtypeStruct((pieces * local_tokens, piece), F32),
            jax.ShapeDtypeStruct((2 * pieces * local_tokens, rows), BF16),
        ),
        in_specs=[whole()] * 6,
        out_specs=(whole(), whole()),
        compiler_params=params,
        name="shared",
    )(normed, shared_gate, shared_up, shared_down, route_expert.T, route_weight.T)

    results = pl.pallas_call(
        functools.partial(expert_kernel, pieces=pieces),
        out_shape=jax.ShapeDtypeStruct((rows, piece), BF16),
        in_specs=[whole()] * 7,
        out_specs=whole(),
        compiler_params=params,
        name="expert",
    )(arrived.reshape(rows, piece), *weights, *others)
    with jax.named_scope("homeward"):
        returned = lax.all_to_all(results.reshape(experts, slots * pieces, piece), "ep", 0, 0, tiled=True)

    mine = pl.pallas_call(
        combine_kernel,
        out_shape=jax.ShapeDtypeStruct((pieces * local_tokens, piece), F32),
        in_specs=[whole()] * 3,
        out_specs=whole(),
        name="combine",
    )(mix, returned.reshape(rows, piece), part)
    other = lax.ppermute(mine, "tp", swap)
    return pl.pallas_call(
        functools.partial(closing_kernel, pieces=pieces),
        out_shape=jax.ShapeDtypeStruct((local_tokens, out_gain.shape[0]), BF16),
        in_specs=[whole()] * 3,
        out_specs=whole(),
        scratch_shapes=[VMEM((pieces * local_tokens, piece), F32)],
        name="closing",
    )(mine, other, out_gain.reshape(1, -1))


def solution(mesh):
    return jax.shard_map(
        body,
        mesh=mesh,
        in_specs=(
            P(("grp", "ep"), None),
            P(),
            P(("grp", "ep"), None),
            P(("grp", "ep"), None),
            P("ep", None, "tp"),
            P("ep", None, "tp"),
            P("ep", "tp", None),
            P(None, "tp"),
            P(None, "tp"),
            P("tp", None),
            P("tp"),
        ),
        out_specs=P(("grp", "ep"), "tp"),
        check_vma=False,
    )
```

time: 103 us -> 93.3 us (0.906)
  Pallas kernels: 0 us -> 13.2 us
  other arithmetic: 8.86 us -> 0 us
  matrix products: 8.8 us -> 0 us
  waiting for transfers between devices: 20.9 us -> 12.1 us
  starting transfers between devices: 28.3 us -> 32.8 us
  blocking collectives: 20 us -> 23.3 us
  local copies, waits for them, and re-layouts: 14.5 us -> 11.3 us
    ppermute x0 -> x4, starting transfers between devices: none -> 24.8 us  [the longest x3 20.9 us: body(): others = tuple((lax.ppermute(w, 'tp', swap) for w in weights))]
    all_to_all x2 -> x1, starting transfers between devices: 28.3 us -> 8.02 us  [body(): lax.all_to_all(results.reshape(experts, slots * pieces, piece), 'ep', 0,...]
    pallas_call x0 -> x5, Pallas kernels: none -> 13.2 us  [the longest x1 5.67 us: body(): pl.pallas_call(functools.partial(expert_kernel, pieces=pieces), out_shape...]
    all_to_all x2 -> x1, waiting for transfers between devices: 20.9 us -> 11.3 us  [body(): lax.all_to_all(results.reshape(experts, slots * pieces, piece), 'ep', 0,...]
    dot_general x4 -> x0, matrix products: 8.8 us -> none  [the longest x1 3.71 us: body(): jnp.dot(swiglu_hidden(expert_rows, gate_weight[0], up_weight[0]), down_we...]
    all_to_all x2 -> x1, blocking collectives: 15.2 us -> 23.3 us  [body(): lax.all_to_all(send.reshape(experts, slots * pieces, piece), 'ep', 0, 0,...]
    unnamed x18 -> x30, local copies, waits for them, and re-layouts: 3.23 us -> 9.4 us
    unnamed x1 -> x0, blocking collectives: 4.82 us -> none
  transfers between devices with their start and end apart: 2 -> 5, of which waited for: 2 -> 2; matrix products, arithmetic and copies ran while one was open for 8% -> 2% of each run, Pallas kernels for 0% -> 4%
where the time goes in v1:
time: 93.3 us; the launch traced here: 92.9 us
  starting transfers between devices  32.8 us (35%)
  blocking collectives  23.3 us (25%)
  Pallas kernels  13.2 us (14%)
  waiting for transfers between devices  12.1 us (13%)
  local copies, waits for them, and re-layouts  11.3 us (12%)
    all_to_all x1, blocking collectives, body(): lax.all_to_all(send.reshape(experts, slots * pieces, piece), 'ep', 0, 0,...  23.3 us
    ppermute x3, starting transfers between devices, body(): others = tuple((lax.ppermute(w, 'tp', swap) for w in weights))  20.9 us
    all_to_all x1, waiting for transfers between devices, body(): lax.all_to_all(results.reshape(experts, slots * pieces, piece), 'ep', 0,...  11.3 us
    unnamed x30, local copies, waits for them, and re-layouts  9.4 us
    all_to_all x1, starting transfers between devices, body(): lax.all_to_all(results.reshape(experts, slots * pieces, piece), 'ep', 0,...  8.02 us
    pallas_call x1, Pallas kernels, body(): pl.pallas_call(functools.partial(expert_kernel, pieces=pieces), out_shape...  5.67 us
    ppermute x1, starting transfers between devices, body(): other = lax.ppermute(mine, 'tp', swap)  3.88 us
    pallas_call x1, Pallas kernels, body(): pl.pallas_call(functools.partial(dispatch_kernel, **sizes), out_shape=(ja...  2.33 us
  transfers between devices with their start and end apart: 5, of which 2 were waited for; matrix products, arithmetic and copies ran while one was open for 2% of the time, Pallas kernels for 4%

profile of v1, /device:TPU:513, one launch (start us, length us, event | category | flops | bytes accessed | tf_op | source)
XLA Modules:
  0.0 92.9 jit_solution(229804169177276283)
XLA Ops:
  0.0 20.4 %collective-permute-start = (bf16[2048,384]{1,0:T(8,128)(2,1)}, bf16[2048,384]{1,0:T(8,128)(2,1)S(1)}, u32[]{:S(2)}, u32[]{:S(2)}) collective-permute-start(bf16[2048,384]{1,0:T(8,128)(2,1)} %bitcast.10), channel_id=1, source_target_pairs={{0,1},{1,0},{2,3},{3,2},{4,5},{5,4},{6,7},{7,6},{8,9},{9,8},{10,11... | collective-permute-start | bytes 4718600 | tf_op jit(solution)/shard_map/ppermute | solution.py:170
  20.4 0.5 collective-permute-start.2
  20.9 1.3 %reshape.18.gain_ref = bf16[1,2048]{1,0:T(2,128)(2,1)} reshape(bf16[2048]{0:T(1024)(128)(2,1)} %param.12) | data formatting | bytes 8192 | tf_op jit(solution)/shard_map/reshape | solution.py:181
  22.2 2.3 %dispatch.1 = (bf16[512,512]{1,0:T(8,128)(2,1)}, bf16[32,2048]{1,0:T(8,128)(2,1)}) custom-call(bf16[32,2048]{1,0:T(8,128)(2,1)} %tokens_ref.1, bf16[1,2048]{1,0:T(2,128)(2,1)} %reshape.18.gain_ref, s32[6,32]{1,0:T(8,128)} %bitcast.16), custom_call_target="tpu_custom_call" | custom-call | tf_op jit(solution)/shard_map/dispatch/pallas_call | solution.py:172
  24.5 23.3 %all_to_all.10 = bf16[64,8,512]{2,1,0:T(8,128)(2,1)S(1)} all-to-all(bf16[64,8,512]{2,1,0:T(8,128)(2,1)} %bitcast.19), channel_id=1, replica_groups=mesh['grp'=2,'ep'=64,'tp'=2] {'ep'}, dimensions={0} | all-to-all | bytes 1048576 | tf_op jit(solution)/shard_map/outward/all_to_all | solution.py:183
  47.9 1.1 %copy-done.11 = bf16[2048,384]{1,0:T(8,128)(2,1)} copy-done((bf16[2048,384]{1,0:T(8,128)(2,1)}, bf16[2048,384]{1,0:T(8,128)(2,1)S(1)}, u32[]{:S(2)}) %copy-start.11) | copy-done | bytes 1572888
  49.0 0.5 copy-done.12
  49.6 1.4 %copy-done = bf16[1,2048,384]{2,1,0:T(8,128)(2,1)S(1)} copy-done((bf16[1,2048,384]{2,1,0:T(8,128)(2,1)S(1)}, bf16[1,2048,384]{2,1,0:T(8,128)(2,1)}, u32[]{:S(2)}) %copy-start) | copy-done | bytes 1572888
  51.0 1.4 %copy-done.1 = bf16[1,2048,384]{2,1,0:T(8,128)(2,1)S(1)} copy-done((bf16[1,2048,384]{2,1,0:T(8,128)(2,1)S(1)}, bf16[1,2048,384]{2,1,0:T(8,128)(2,1)}, u32[]{:S(2)}) %copy-start.1) | copy-done | bytes 1572888
  52.4 1.4 %copy-done.2 = bf16[1,384,2048]{2,1,0:T(8,128)(2,1)S(1)} copy-done((bf16[1,384,2048]{2,1,0:T(8,128)(2,1)S(1)}, bf16[1,384,2048]{2,1,0:T(8,128)(2,1)}, u32[]{:S(2)}) %copy-start.2) | copy-done | bytes 1572888
  53.8 5.7 %expert.1 = bf16[512,512]{1,0:T(8,128)(2,1)} custom-call(bf16[512,512]{1,0:T(8,128)(2,1)S(1)} %bitcast.9, bf16[2048,384]{1,0:T(8,128)(2,1)S(1)} %bitcast.11, bf16[2048,384]{1,0:T(8,128)(2,1)S(1)} %bitcast.13, bf16[384,2048]{1,0:T(8,128)(2,1)S(1)} %bitcast.15, bf16[2048,384]{1,0:T(8,128)(2,1)} %copy-done.11, bf16[2048,384]{1,0:T(8,128)(2,1)} %copy-done.12, ...), custom_call_target="tpu_custom_call" | custom-call | tf_op jit(solution)/shard_map/expert/pallas_call | solution.py:197
  59.5 8.0 %all-to-all-start.1 = ((bf16[64,8,512]{2,1,0:T(8,128)(2,1)}), bf16[64,8,512]{2,1,0:T(8,128)(2,1)}, u32[]{:S(2)}, u32[]{:S(2)}) async-start(bf16[64,8,512]{2,1,0:T(8,128)(2,1)} %bitcast.7), calls=%async_computation.1 | async-start | bytes 1048576 | tf_op jit(solution)/shard_map/homeward/all_to_all | solution.py:206
  67.5 0.0 copy-start.5
  67.6 1.4 %copy-done.5 = bf16[384,2048]{1,0:T(8,128)(2,1)S(1)} copy-done((bf16[384,2048]{1,0:T(8,128)(2,1)S(1)}, bf16[384,2048]{1,0:T(8,128)(2,1)}, u32[]{:S(2)}) %copy-start.5) | copy-done | bytes 1572888
  69.0 1.3 %shared.1 = (f32[128,512]{1,0:T(8,128)S(1)}, bf16[256,512]{1,0:T(8,128)(2,1)S(1)}) custom-call(bf16[32,2048]{1,0:T(8,128)(2,1)S(1)} %copy-done.8, bf16[2048,384]{1,0:T(8,128)(2,1)S(1)} %copy-done.3, bf16[2048,384]{1,0:T(8,128)(2,1)S(1)} %copy-done.4, bf16[384,2048]{1,0:T(8,128)(2,1)S(1)} %copy-done.5, s32[6,32]{1,0:T(8,128)S(1)} %bitcast.17, ...), custom_call_target="tpu_custom_call" | custom-call | tf_op jit(solution)/shard_map/shared/pallas_call | solution.py:185
  70.2 0.7 copy-done.6
  70.9 0.7 copy-done.7
  71.6 11.3 %all-to-all-done.1 = bf16[64,8,512]{2,1,0:T(8,128)(2,1)} async-done(((bf16[64,8,512]{2,1,0:T(8,128)(2,1)}), bf16[64,8,512]{2,1,0:T(8,128)(2,1)}, u32[]{:S(2)}, u32[]{:S(2)}) %all-to-all-start.1) | async-done | bytes 524320 | tf_op jit(solution)/shard_map/homeward/all_to_all | solution.py:206
  83.0 2.2 %combine.1.mine_ref = f32[128,512]{1,0:T(8,128)} custom-call(bf16[256,512]{1,0:T(8,128)(2,1)} %copy-done.7, bf16[512,512]{1,0:T(8,128)(2,1)} %bitcast.8.returned_ref, f32[128,512]{1,0:T(8,128)} %copy-done.6), custom_call_target="tpu_custom_call" | custom-call | tf_op jit(solution)/shard_map/combine/pallas_call | solution.py:208
  85.1 3.9 %collective-permute-start.3 = (f32[128,512]{1,0:T(8,128)}, f32[128,512]{1,0:T(8,128)S(1)}, u32[]{:S(2)}, u32[]{:S(2)}) collective-permute-start(f32[128,512]{1,0:T(8,128)} %combine.1.mine_ref), channel_id=1, source_target_pairs={{0,1},{1,0},{2,3},{3,2},{4,5},{5,4},{6,7},{7,6},{8,9},{9,8},{10,11... | collective-permute-start | bytes 786440 | tf_op jit(solution)/shard_map/ppermute | solution.py:215
  89.0 0.6 reshape.23.gain_ref
  89.6 0.8 collective-permute-done.3.other_ref
  90.4 0.7 copy-done.13
  91.1 1.8 %closing.1 = bf16[32,1024]{1,0:T(8,128)(2,1)} custom-call(f32[128,512]{1,0:T(8,128)} %combine.1.mine_ref, f32[128,512]{1,0:T(8,128)} %copy-done.13, bf16[1,1024]{1,0:T(2,128)(2,1)} %reshape.23.gain_ref), custom_call_target="tpu_custom_call" | custom-call | tf_op jit(solution)/shard_map/closing/pallas_call | solution.py:216
  (24 shorter events, 0.0 us)
Async XLA Ops:
  0.0 47.9 %collective-permute-start = (bf16[2048,384]{1,0:T(8,128)(2,1)}, bf16[2048,384]{1,0:T(8,128)(2,1)S(1)}, u32[]{:S(2)}, u32[]{:S(2)}) collective-permute-start(bf16[2048,384]{1,0:T(8,128)(2,1)} %bitcast.10), channel_id=1, source_target_pairs={{0,1},{1,0},{2,3},{3,2},{4,5},{5,4},{6,7},{7,6},{8,9},{9,8},{10,11... | collective-permute-start | bytes 4718600 | tf_op jit(solution)/shard_map/ppermute | solution.py:170
  20.4 27.5 %collective-permute-start.1 = (bf16[2048,384]{1,0:T(8,128)(2,1)}, bf16[2048,384]{1,0:T(8,128)(2,1)S(1)}, u32[]{:S(2)}, u32[]{:S(2)}) collective-permute-start(bf16[2048,384]{1,0:T(8,128)(2,1)} %bitcast.12), channel_id=1, source_target_pairs={{0,1},{1,0},{2,3},{3,2},{4,5},{5,4},{6,7},{7,6},{8,9},{9,8},{10,11... | collective-permute-start | bytes 4718600 | tf_op jit(solution)/shard_map/ppermute | solution.py:170
  20.4 27.5 %collective-permute-start.2 = (bf16[384,2048]{1,0:T(8,128)(2,1)}, bf16[384,2048]{1,0:T(8,128)(2,1)}, u32[]{:S(2)}, u32[]{:S(2)}) collective-permute-start(bf16[384,2048]{1,0:T(8,128)(2,1)} %bitcast.14), channel_id=1, source_target_pairs={{0,1},{1,0},{2,3},{3,2},{4,5},{5,4},{6,7},{7,6},{8,9},{9,8},{10,11... | collective-permute-start | bytes 4718600 | tf_op jit(solution)/shard_map/ppermute | solution.py:170
  47.9 1.1 %copy-start.11 = (bf16[2048,384]{1,0:T(8,128)(2,1)}, bf16[2048,384]{1,0:T(8,128)(2,1)S(1)}, u32[]{:S(2)}) copy-start(bf16[2048,384]{1,0:T(8,128)(2,1)S(1)} %collective-permute-done.gate2_ref) | copy-start | bytes 4718596
  47.9 1.7 %copy-start.12 = (bf16[2048,384]{1,0:T(8,128)(2,1)}, bf16[2048,384]{1,0:T(8,128)(2,1)S(1)}, u32[]{:S(2)}) copy-start(bf16[2048,384]{1,0:T(8,128)(2,1)S(1)} %collective-permute-done.1.up2_ref) | copy-start | bytes 4718596
  49.6 1.4 %copy-start = (bf16[1,2048,384]{2,1,0:T(8,128)(2,1)S(1)}, bf16[1,2048,384]{2,1,0:T(8,128)(2,1)}, u32[]{:S(2)}) copy-start(bf16[1,2048,384]{2,1,0:T(8,128)(2,1)} %param.15) | copy-start | bytes 4718596
  51.0 1.4 %copy-start.1 = (bf16[1,2048,384]{2,1,0:T(8,128)(2,1)S(1)}, bf16[1,2048,384]{2,1,0:T(8,128)(2,1)}, u32[]{:S(2)}) copy-start(bf16[1,2048,384]{2,1,0:T(8,128)(2,1)} %param.16) | copy-start | bytes 4718596
  52.4 1.4 %copy-start.2 = (bf16[1,384,2048]{2,1,0:T(8,128)(2,1)S(1)}, bf16[1,384,2048]{2,1,0:T(8,128)(2,1)}, u32[]{:S(2)}) copy-start(bf16[1,384,2048]{2,1,0:T(8,128)(2,1)} %param.17) | copy-start | bytes 4718596
  53.8 13.7 %copy-start.3 = (bf16[2048,384]{1,0:T(8,128)(2,1)S(1)}, bf16[2048,384]{1,0:T(8,128)(2,1)}, u32[]{:S(2)}) copy-start(bf16[2048,384]{1,0:T(8,128)(2,1)} %gate_ref.1) | copy-start | bytes 4718596
  53.8 13.7 %copy-start.4 = (bf16[2048,384]{1,0:T(8,128)(2,1)S(1)}, bf16[2048,384]{1,0:T(8,128)(2,1)}, u32[]{:S(2)}) copy-start(bf16[2048,384]{1,0:T(8,128)(2,1)} %up_ref.1) | copy-start | bytes 4718596
  53.8 13.7 %copy-start.8 = (bf16[32,2048]{1,0:T(8,128)(2,1)S(1)}, bf16[32,2048]{1,0:T(8,128)(2,1)}, u32[]{:S(2)}) copy-start(bf16[32,2048]{1,0:T(8,128)(2,1)} %get-tuple-element.9.normed_ref) | copy-start | bytes 393220
  53.8 13.7 %copy-start.9 = (s32[32,6]{0,1:T(8,128)S(1)}, s32[32,6]{0,1:T(8,128)}, u32[]{:S(2)}) copy-start(s32[32,6]{0,1:T(8,128)} %param.13) | copy-start | bytes 2308
  53.8 13.7 %copy-start.10 = (f32[32,6]{0,1:T(8,128)S(1)}, f32[32,6]{0,1:T(8,128)}, u32[]{:S(2)}) copy-start(f32[32,6]{0,1:T(8,128)} %param.14) | copy-start | bytes 2308
  59.5 23.5 %all-to-all-start.1 = ((bf16[64,8,512]{2,1,0:T(8,128)(2,1)}), bf16[64,8,512]{2,1,0:T(8,128)(2,1)}, u32[]{:S(2)}, u32[]{:S(2)}) async-start(bf16[64,8,512]{2,1,0:T(8,128)(2,1)} %bitcast.7), calls=%async_computation.1 | async-start | bytes 1048576 | tf_op jit(solution)/shard_map/homeward/all_to_all | solution.py:206
  67.5 1.4 %copy-start.5 = (bf16[384,2048]{1,0:T(8,128)(2,1)S(1)}, bf16[384,2048]{1,0:T(8,128)(2,1)}, u32[]{:S(2)}) copy-start(bf16[384,2048]{1,0:T(8,128)(2,1)} %down_ref.1) | copy-start | bytes 4718596
  69.0 20.1 %copy-start.14 = (bf16[1024]{0:T(1024)(128)(2,1)S(1)}, bf16[1024]{0:T(1024)(128)(2,1)}, u32[]{:S(2)}) copy-start(bf16[1024]{0:T(1024)(128)(2,1)} %param.21) | copy-start | bytes 6148
  70.2 0.7 copy-start.6
  70.9 0.7 copy-start.7
  85.1 5.3 %collective-permute-start.3 = (f32[128,512]{1,0:T(8,128)}, f32[128,512]{1,0:T(8,128)S(1)}, u32[]{:S(2)}, u32[]{:S(2)}) collective-permute-start(f32[128,512]{1,0:T(8,128)} %combine.1.mine_ref), channel_id=1, source_target_pairs={{0,1},{1,0},{2,3},{3,2},{4,5},{5,4},{6,7},{7,6},{8,9},{9,8},{10,11... | collective-permute-start | bytes 786440 | tf_op jit(solution)/shard_map/ppermute | solution.py:215
  90.4 0.7 copy-start.13

commit v2 on v1

--- a/solution.py
+++ b/solution.py
@@ -15,6 +15,22 @@
 
 def whole():
     return pl.BlockSpec(memory_space=VMEM)
+
+
+def anywhere():
+    return pl.BlockSpec(memory_space=pl.ANY)
+
+
+def held(*arrays):
+    return [pltpu.with_memory_space_constraint(a, VMEM) for a in arrays]
+
+
+def far(*arrays):
+    return [pltpu.with_memory_space_constraint(a, pltpu.HBM) for a in arrays]
+
+
+def grant(mebibytes):
+    return pltpu.CompilerParams(vmem_limit_bytes=mebibytes * 1024 * 1024)
 
 
 def iota(shape, dim):
@@ -44,15 +60,40 @@
     return jnp.where(keep, total, 0.0)
 
 
-def dispatch_kernel(tokens_ref, gain_ref, route_ref, send_ref, normed_ref, *, slots, pieces, experts):
+def dispatch_kernel(
+    tokens_hbm,
+    gain_hbm,
+    route_hbm,
+    send_ref,
+    normed_ref,
+    tokens_ref,
+    gain_ref,
+    route_ref,
+    sems,
+    *,
+    slots,
+    pieces,
+    experts,
+):
     core = lax.axis_index("tp")
+    loads = [
+        pltpu.make_async_copy(src, dst, sems.at[i])
+        for i, (src, dst) in enumerate(
+            ((route_hbm, route_ref), (tokens_hbm, tokens_ref), (gain_hbm, gain_ref))
+        )
+    ]
+    for load in loads:
+        load.start()
+    loads[0].wait()
+    pick = chosen(route_ref[...], core, slots, pieces, experts).astype(BF16)
+    loads[1].wait()
+    loads[2].wait()
     values = tokens_ref[...].astype(F32)
     scaled = values * lax.rsqrt(jnp.mean(values * values, axis=-1, keepdims=True) + EPSILON)
-    normed = (scaled * gain_ref[...].astype(F32)).astype(BF16)
+    normed = (scaled * gain_ref[...].astype(F32)[None, :]).astype(BF16)
     normed_ref[...] = normed
     piece = normed.shape[1] // pieces
     stacked = jnp.concatenate([normed[:, q * piece : (q + 1) * piece] for q in range(pieces)], axis=0)
-    pick = chosen(route_ref[...], core, slots, pieces, experts).astype(BF16)
     send_ref[...] = jnp.dot(pick, stacked, preferred_element_type=F32).astype(BF16)
 
 
@@ -81,8 +122,27 @@
 
 
 def expert_kernel(
-    rows_ref, gate_ref, up_ref, down_ref, gate2_ref, up2_ref, down2_ref, out_ref, *, pieces
+    rows_ref,
+    gate2_ref,
+    up2_ref,
+    down2_ref,
+    gate_hbm,
+    up_hbm,
+    down_hbm,
+    out_ref,
+    gate_ref,
+    up_ref,
+    down_ref,
+    sems,
+    *,
+    pieces,
 ):
+    loads = [
+        pltpu.make_async_copy(src, dst, sems.at[i])
+        for i, (src, dst) in enumerate(((gate_hbm, gate_ref), (up_hbm, up_ref), (down_hbm, down_ref)))
+    ]
+    for load in loads:
+        load.start()
     total = rows_ref.shape[0]
     rows, block = total // pieces, total // 2
     half = rows // 2
@@ -100,18 +160,22 @@
         axis=1,
     )
     hidden = []
-    for g, u in ((gate_ref, up_ref), (gate2_ref, up2_ref)):
+    for own, (g, u) in enumerate(((gate2_ref, up2_ref), (gate_ref, up_ref))):
+        if own:
+            loads[0].wait()
+            loads[1].wait()
         gate = jnp.dot(inputs, g[...], preferred_element_type=F32)
         upward = jnp.dot(inputs, u[...], preferred_element_type=F32)
         hidden.append((gate * jax.nn.sigmoid(gate) * upward).astype(BF16))
     back = order.T
+    loads[2].wait()
     results = []
     for q in range(pieces):
         span = slice(q * piece, (q + 1) * piece)
         results.append(
             (
-                jnp.dot(hidden[0], down_ref[:, span], preferred_element_type=F32)
-                + jnp.dot(hidden[1], down2_ref[:, span], preferred_element_type=F32)
+                jnp.dot(hidden[0], down2_ref[:, span], preferred_element_type=F32)
+                + jnp.dot(hidden[1], down_ref[:, span], preferred_element_type=F32)
             ).astype(BF16)
         )
     for h in range(2):
@@ -134,7 +198,7 @@
     squares = functools.reduce(jnp.add, [squares[q * tokens : (q + 1) * tokens] for q in range(pieces)])
     scale = lax.rsqrt(squares / (pieces * piece) + EPSILON)
     mine = out_ref.shape[1] // piece
-    gain = gain_ref[...].astype(F32)
+    gain = gain_ref[...].astype(F32)[None, :]
     for q in range(mine):
         start = pl.multiple_of((core * mine + q) * tokens, 8)
         values = total_ref[pl.ds(start, tokens), :] * scale
@@ -163,7 +227,6 @@
     piece = width // pieces
     rows = experts * slots * pieces
     sizes = dict(slots=slots, pieces=pieces, experts=experts)
-    params = pltpu.CompilerParams(vmem_limit_bytes=48 * 1024 * 1024)
 
     swap = [(i, (i + 1) % cores) for i in range(cores)]
     weights = (gate_weight[0], up_weight[0], down_weight[0])
@@ -172,46 +235,55 @@
     send, normed = pl.pallas_call(
         functools.partial(dispatch_kernel, **sizes),
         out_shape=(
-            jax.ShapeDtypeStruct((rows, piece), BF16),
-            jax.ShapeDtypeStruct((local_tokens, width), BF16),
+            VMEM((rows, piece), BF16),
+            VMEM((local_tokens, width), BF16),
         ),
-        in_specs=[whole()] * 3,
+        in_specs=[anywhere()] * 3,
         out_specs=(whole(), whole()),
+        scratch_shapes=[
+            VMEM(tokens.shape, BF16),
+            VMEM(in_gain.shape, BF16),
+            VMEM(route_expert.shape[::-1], jnp.int32),
+            pltpu.SemaphoreType.DMA((3,)),
+        ],
+        compiler_params=grant(6),
         name="dispatch",
-    )(tokens, in_gain.reshape(1, width), route_expert.T)
+    )(*far(tokens, in_gain, route_expert.T))
     with jax.named_scope("outward"):
         arrived = lax.all_to_all(send.reshape(experts, slots * pieces, piece), "ep", 0, 0, tiled=True)
 
     part, mix = pl.pallas_call(
         functools.partial(shared_kernel, **sizes),
         out_shape=(
-            jax.ShapeDtypeStruct((pieces * local_tokens, piece), F32),
-            jax.ShapeDtypeStruct((2 * pieces * local_tokens, rows), BF16),
+            VMEM((pieces * local_tokens, piece), F32),
+            VMEM((2 * pieces * local_tokens, rows), BF16),
         ),
         in_specs=[whole()] * 6,
         out_specs=(whole(), whole()),
-        compiler_params=params,
+        compiler_params=grant(8),
         name="shared",
-    )(normed, shared_gate, shared_up, shared_down, route_expert.T, route_weight.T)
+    )(*held(normed, shared_gate, shared_up, shared_down, route_expert.T, route_weight.T))
 
     results = pl.pallas_call(
         functools.partial(expert_kernel, pieces=pieces),
-        out_shape=jax.ShapeDtypeStruct((rows, piece), BF16),
-        in_specs=[whole()] * 7,
+        out_shape=VMEM((rows, piece), BF16),
+        in_specs=[whole()] * 4 + [anywhere()] * 3,
         out_specs=whole(),
-        compiler_params=params,
+        scratch_shapes=[VMEM(w.shape, BF16) for w in weights] + [pltpu.SemaphoreType.DMA((3,))],
+        compiler_params=grant(12),
         name="expert",
-    )(arrived.reshape(rows, piece), *weights, *others)
+    )(*held(arrived.reshape(rows, piece), *others), *far(*weights))
     with jax.named_scope("homeward"):
         returned = lax.all_to_all(results.reshape(experts, slots * pieces, piece), "ep", 0, 0, tiled=True)
 
     mine = pl.pallas_call(
         combine_kernel,
-        out_shape=jax.ShapeDtypeStruct((pieces * local_tokens, piece), F32),
+        out_shape=VMEM((pieces * local_tokens, piece), F32),
         in_specs=[whole()] * 3,
         out_specs=whole(),
+        compiler_params=grant(4),
         name="combine",
-    )(mix, returned.reshape(rows, piece), part)
+    )(*held(mix, returned.reshape(rows, piece), part))
     other = lax.ppermute(mine, "tp", swap)
     return pl.pallas_call(
         functools.partial(closing_kernel, pieces=pieces),
@@ -219,8 +291,9 @@
         in_specs=[whole()] * 3,
         out_specs=whole(),
         scratch_shapes=[VMEM((pieces * local_tokens, piece), F32)],
+        compiler_params=grant(4),
         name="closing",
-    )(mine, other, out_gain.reshape(1, -1))
+    )(*held(mine, other, out_gain))
 
 
 def solution(mesh):

time: 93.3 us -> 80 us (0.86)
  local copies, waits for them, and re-layouts: 11.3 us -> 2.83 us
  Pallas kernels: 13.2 us -> 8.95 us
    unnamed x30 -> x12, local copies, waits for them, and re-layouts: 9.4 us -> 2.83 us
    pallas_call x3, Pallas kernels: 5.78 us -> 3.05 us  [the longest x1 1.48 us: body(): pl.pallas_call(functools.partial(dispatch_kernel, **sizes), out_shape=(VM...]
    reshape x2 -> x0, local copies, waits for them, and re-layouts: 1.88 us -> none  [the longest x1 1.29 us: body(): in_gain.reshape(1, width)]
    pallas_call x1, Pallas kernels: 1.78 us -> 0.76 us  [body(): pl.pallas_call(functools.partial(closing_kernel, pieces=pieces), out_shap...]
  transfers between devices with their start and end apart: 5 -> 5, of which waited for: 2 -> 2; matrix products, arithmetic and copies ran while one was open for 2% -> 0% of each run, Pallas kernels for 4% -> 3%
where the time goes in v2:
time: 80 us; the launch traced here: 79.7 us
  starting transfers between devices  32.8 us (41%)
  blocking collectives  22.4 us (28%)
  waiting for transfers between devices  12.6 us (16%)
  Pallas kernels  8.95 us (11%)
  local copies, waits for them, and re-layouts  2.83 us (4%)
    all_to_all x1, blocking collectives, body(): lax.all_to_all(send.reshape(experts, slots * pieces, piece), 'ep', 0, 0,...  22.4 us
    ppermute x3, starting transfers between devices, body(): others = tuple((lax.ppermute(w, 'tp', swap) for w in weights))  20.9 us
    all_to_all x1, waiting for transfers between devices, body(): lax.all_to_all(results.reshape(experts, slots * pieces, piece), 'ep', 0,...  11.4 us
    all_to_all x1, starting transfers between devices, body(): lax.all_to_all(results.reshape(experts, slots * pieces, piece), 'ep', 0,...  8.04 us
    pallas_call x1, Pallas kernels, body(): pl.pallas_call(functools.partial(expert_kernel, pieces=pieces), out_shape...  5.15 us
    ppermute x1, starting transfers between devices, body(): other = lax.ppermute(mine, 'tp', swap)  3.87 us
    unnamed x12, local copies, waits for them, and re-layouts  2.83 us
  transfers between devices with their start and end apart: 5, of which 2 were waited for; matrix products, arithmetic and copies ran while one was open for 0% of the time, Pallas kernels for 3%

profile of v2, /device:TPU:513, one launch (start us, length us, event | category | flops | bytes accessed | tf_op | source)
XLA Modules:
  0.0 79.7 jit_solution(7835849974662702804)
XLA Ops:
  0.0 20.4 %collective-permute-start = (bf16[2048,384]{1,0:T(8,128)(2,1)}, bf16[2048,384]{1,0:T(8,128)(2,1)S(1)}, u32[]{:S(2)}, u32[]{:S(2)}) collective-permute-start(bf16[2048,384]{1,0:T(8,128)(2,1)} %bitcast.15), channel_id=1, source_target_pairs={{0,1},{1,0},{2,3},{3,2},{4,5},{5,4},{6,7},{7,6},{8,9},{9,8},{10,11... | collective-permute-start | bytes 4718600 | tf_op jit(solution)/shard_map/ppermute | solution.py:233
  20.4 0.0 collective-permute-start.1
  20.4 0.5 collective-permute-start.2
  20.9 1.5 %dispatch.1 = (bf16[512,512]{1,0:T(8,128)(2,1)S(1)}, bf16[32,2048]{1,0:T(8,128)(2,1)S(1)}) custom-call(bf16[32,2048]{1,0:T(8,128)(2,1)} %tokens_hbm.1, bf16[2048]{0:T(1024)(128)(2,1)} %gain_hbm.1, s32[6,32]{1,0:T(8,128)} %bitcast.12), custom_call_target="tpu_custom_call" | custom-call | tf_op jit(solution)/shard_map/dispatch/pallas_call | solution.py:235
  22.4 22.4 %all_to_all.10 = bf16[64,8,512]{2,1,0:T(8,128)(2,1)S(1)} all-to-all(bf16[64,8,512]{2,1,0:T(8,128)(2,1)S(1)} %bitcast.11), channel_id=1, replica_groups=mesh['grp'=2,'ep'=64,'tp'=2] {'ep'}, dimensions={0} | all-to-all | bytes 1048576 | tf_op jit(solution)/shard_map/outward/all_to_all | solution.py:253
  44.9 0.0 collective-permute-done.gate2_ref
  44.9 0.0 collective-permute-done.1.up2_ref
  44.9 0.0 collective-permute-done.2.down2_ref
  44.9 0.0 copy-start
  44.9 0.0 copy-start.3
  44.9 0.0 copy-start.4
  44.9 5.1 %expert.1 = bf16[512,512]{1,0:T(8,128)(2,1)} custom-call(bf16[512,512]{1,0:T(8,128)(2,1)S(1)} %bitcast.9, bf16[2048,384]{1,0:T(8,128)(2,1)S(1)} %collective-permute-done.gate2_ref, bf16[2048,384]{1,0:T(8,128)(2,1)S(1)} %collective-permute-done.1.up2_ref, bf16[384,2048]{1,0:T(8,128)(2,1)S(1)} %collective-permute-done.2.down2_ref, bf16[2048,384]{1,0:T(8,128)(2,1)} %bitcast.16, ...), custom_call_target="tpu_custom_call" | custom-call | tf_op jit(solution)/shard_map/expert/pallas_call | solution.py:267
  50.1 8.0 %all-to-all-start.1 = ((bf16[64,8,512]{2,1,0:T(8,128)(2,1)}), bf16[64,8,512]{2,1,0:T(8,128)(2,1)S(1)}, u32[]{:S(2)}, u32[]{:S(2)}) async-start(bf16[64,8,512]{2,1,0:T(8,128)(2,1)} %bitcast.7), calls=%async_computation.1 | async-start | bytes 1048576 | tf_op jit(solution)/shard_map/homeward/all_to_all | solution.py:277
  58.1 0.0 copy-done
  58.1 0.0 copy-done.3
  58.1 0.0 copy-start.1
  58.1 1.4 %copy-done.1 = bf16[2048,384]{1,0:T(8,128)(2,1)S(1)} copy-done((bf16[2048,384]{1,0:T(8,128)(2,1)S(1)}, bf16[2048,384]{1,0:T(8,128)(2,1)}, u32[]{:S(2)}) %copy-start.1) | copy-done | bytes 1572888
  59.5 1.4 %copy-done.2 = bf16[384,2048]{1,0:T(8,128)(2,1)S(1)} copy-done((bf16[384,2048]{1,0:T(8,128)(2,1)S(1)}, bf16[384,2048]{1,0:T(8,128)(2,1)}, u32[]{:S(2)}) %copy-start.2) | copy-done | bytes 1572888
  61.0 1.3 %shared.1 = (f32[128,512]{1,0:T(8,128)S(1)}, bf16[256,512]{1,0:T(8,128)(2,1)S(1)}) custom-call(bf16[32,2048]{1,0:T(8,128)(2,1)S(1)} %get-tuple-element.9.normed_ref, bf16[2048,384]{1,0:T(8,128)(2,1)S(1)} %copy-done, bf16[2048,384]{1,0:T(8,128)(2,1)S(1)} %copy-done.1, bf16[384,2048]{1,0:T(8,128)(2,1)S(1)} %copy-done.2, s32[6,32]{1,0:T(8,128)S(1)} %bitcast.13, ...), custom_call_target="tpu_custom_call" | custom-call | tf_op jit(solution)/shard_map/shared/pallas_call | solution.py:255
  62.2 11.4 %all-to-all-done.1 = bf16[64,8,512]{2,1,0:T(8,128)(2,1)S(1)} async-done(((bf16[64,8,512]{2,1,0:T(8,128)(2,1)}), bf16[64,8,512]{2,1,0:T(8,128)(2,1)S(1)}, u32[]{:S(2)}, u32[]{:S(2)}) %all-to-all-start.1) | async-done | bytes 524320 | tf_op jit(solution)/shard_map/homeward/all_to_all | solution.py:277
  73.6 0.3 combine.1.mine_ref
  73.9 3.9 %collective-permute-start.3 = (f32[128,512]{1,0:T(8,128)S(1)}, f32[128,512]{1,0:T(8,128)S(1)}, u32[]{:S(2)}, u32[]{:S(2)}) collective-permute-start(f32[128,512]{1,0:T(8,128)S(1)} %combine.1.mine_ref), channel_id=1, source_target_pairs={{0,1},{1,0},{2,3},{3,2},{4,5},{5,4},{6,7},{7,6},{8,9},{9,8},{10,11... | collective-permute-start | bytes 786440 | tf_op jit(solution)/shard_map/ppermute | solution.py:287
  77.8 1.2 %collective-permute-done.3.other_ref = f32[128,512]{1,0:T(8,128)S(1)} collective-permute-done((f32[128,512]{1,0:T(8,128)S(1)}, f32[128,512]{1,0:T(8,128)S(1)}, u32[]{:S(2)}, u32[]{:S(2)}) %collective-permute-start.3) | collective-permute-done | bytes 262176 | tf_op jit(solution)/shard_map/ppermute | solution.py:287
  79.0 0.8 closing.1
  (4 shorter events, 0.0 us)
Async XLA Ops:
  0.0 44.9 %collective-permute-start = (bf16[2048,384]{1,0:T(8,128)(2,1)}, bf16[2048,384]{1,0:T(8,128)(2,1)S(1)}, u32[]{:S(2)}, u32[]{:S(2)}) collective-permute-start(bf16[2048,384]{1,0:T(8,128)(2,1)} %bitcast.15), channel_id=1, source_target_pairs={{0,1},{1,0},{2,3},{3,2},{4,5},{5,4},{6,7},{7,6},{8,9},{9,8},{10,11... | collective-permute-start | bytes 4718600 | tf_op jit(solution)/shard_map/ppermute | solution.py:233
  20.4 24.4 %collective-permute-start.1 = (bf16[2048,384]{1,0:T(8,128)(2,1)}, bf16[2048,384]{1,0:T(8,128)(2,1)S(1)}, u32[]{:S(2)}, u32[]{:S(2)}) collective-permute-start(bf16[2048,384]{1,0:T(8,128)(2,1)} %bitcast.17), channel_id=1, source_target_pairs={{0,1},{1,0},{2,3},{3,2},{4,5},{5,4},{6,7},{7,6},{8,9},{9,8},{10,11... | collective-permute-start | bytes 4718600 | tf_op jit(solution)/shard_map/ppermute | solution.py:233
  20.4 24.4 %collective-permute-start.2 = (bf16[384,2048]{1,0:T(8,128)(2,1)}, bf16[384,2048]{1,0:T(8,128)(2,1)S(1)}, u32[]{:S(2)}, u32[]{:S(2)}) collective-permute-start(bf16[384,2048]{1,0:T(8,128)(2,1)} %bitcast.19), channel_id=1, source_target_pairs={{0,1},{1,0},{2,3},{3,2},{4,5},{5,4},{6,7},{7,6},{8,9},{9,8},{10,11... | collective-permute-start | bytes 4718600 | tf_op jit(solution)/shard_map/ppermute | solution.py:233
  44.9 13.2 %copy-start = (bf16[2048,384]{1,0:T(8,128)(2,1)S(1)}, bf16[2048,384]{1,0:T(8,128)(2,1)}, u32[]{:S(2)}) copy-start(bf16[2048,384]{1,0:T(8,128)(2,1)} %gate_ref.1) | copy-start | bytes 4718596
  44.9 13.2 %copy-start.3 = (s32[32,6]{0,1:T(8,128)S(1)}, s32[32,6]{0,1:T(8,128)}, u32[]{:S(2)}) copy-start(s32[32,6]{0,1:T(8,128)} %param.13) | copy-start | bytes 2308
  44.9 13.2 %copy-start.4 = (f32[32,6]{0,1:T(8,128)S(1)}, f32[32,6]{0,1:T(8,128)}, u32[]{:S(2)}) copy-start(f32[32,6]{0,1:T(8,128)} %param.14) | copy-start | bytes 2308
  50.1 23.6 %all-to-all-start.1 = ((bf16[64,8,512]{2,1,0:T(8,128)(2,1)}), bf16[64,8,512]{2,1,0:T(8,128)(2,1)S(1)}, u32[]{:S(2)}, u32[]{:S(2)}) async-start(bf16[64,8,512]{2,1,0:T(8,128)(2,1)} %bitcast.7), calls=%async_computation.1 | async-start | bytes 1048576 | tf_op jit(solution)/shard_map/homeward/all_to_all | solution.py:277
  58.1 1.4 %copy-start.1 = (bf16[2048,384]{1,0:T(8,128)(2,1)S(1)}, bf16[2048,384]{1,0:T(8,128)(2,1)}, u32[]{:S(2)}) copy-start(bf16[2048,384]{1,0:T(8,128)(2,1)} %up_ref.1) | copy-start | bytes 4718596
  59.5 1.4 %copy-start.2 = (bf16[384,2048]{1,0:T(8,128)(2,1)S(1)}, bf16[384,2048]{1,0:T(8,128)(2,1)}, u32[]{:S(2)}) copy-start(bf16[384,2048]{1,0:T(8,128)(2,1)} %down_ref.1) | copy-start | bytes 4718596
  61.0 18.0 %copy-start.5 = (bf16[1024]{0:T(1024)(128)(2,1)S(1)}, bf16[1024]{0:T(1024)(128)(2,1)}, u32[]{:S(2)}) copy-start(bf16[1024]{0:T(1024)(128)(2,1)} %gain_ref.1) | copy-start | bytes 6148
  73.9 5.0 %collective-permute-start.3 = (f32[128,512]{1,0:T(8,128)S(1)}, f32[128,512]{1,0:T(8,128)S(1)}, u32[]{:S(2)}, u32[]{:S(2)}) collective-permute-start(f32[128,512]{1,0:T(8,128)S(1)} %combine.1.mine_ref), channel_id=1, source_target_pairs={{0,1},{1,0},{2,3},{3,2},{4,5},{5,4},{6,7},{7,6},{8,9},{9,8},{10,11... | collective-permute-start | bytes 786440 | tf_op jit(solution)/shard_map/ppermute | solution.py:287

commit v3 on v2

--- a/solution.py
+++ b/solution.py
@@ -97,25 +97,6 @@
     send_ref[...] = jnp.dot(pick, stacked, preferred_element_type=F32).astype(BF16)
 
 
-def shared_kernel(
-    normed_ref, gate_ref, up_ref, down_ref, route_ref, weight_ref, part_ref, mix_ref, *, slots, pieces, experts
-):
-    core = lax.axis_index("tp")
-    normed = normed_ref[...]
-    gate = jnp.dot(normed, gate_ref[...], preferred_element_type=F32)
-    upward = jnp.dot(normed, up_ref[...], preferred_element_type=F32)
-    hidden = (gate * jax.nn.sigmoid(gate) * upward).astype(BF16)
-    tokens, piece = normed.shape[0], normed.shape[1] // pieces
-    for q in range(pieces):
-        part_ref[q * tokens : (q + 1) * tokens, :] = jnp.dot(
-            hidden, down_ref[:, q * piece : (q + 1) * piece], preferred_element_type=F32
-        )
-    mix = chosen(route_ref[...], core, slots, pieces, experts, weight_ref[...]).T
-    high = mix.astype(BF16)
-    mix_ref[: mix.shape[0], :] = high
-    mix_ref[mix.shape[0] :, :] = (mix - high.astype(F32)).astype(BF16)
-
-
 def gathering(half, pieces):
     to, frm = iota((half * pieces, half * pieces), 0), iota((half * pieces, half * pieces), 1)
     return jnp.where(frm == (to % half) * pieces + to // half, 1.0, 0.0).astype(BF16)
@@ -123,23 +104,50 @@
 
 def expert_kernel(
     rows_ref,
+    normed_ref,
     gate2_ref,
     up2_ref,
     down2_ref,
     gate_hbm,
     up_hbm,
     down_hbm,
+    shared_gate_hbm,
+    shared_up_hbm,
+    shared_down_hbm,
+    route_hbm,
+    weight_hbm,
     out_ref,
+    part_ref,
+    mix_ref,
     gate_ref,
     up_ref,
     down_ref,
+    shared_gate_ref,
+    shared_up_ref,
+    shared_down_ref,
+    route_ref,
+    weight_ref,
     sems,
     *,
+    slots,
     pieces,
+    experts,
 ):
+    core = lax.axis_index("tp")
     loads = [
         pltpu.make_async_copy(src, dst, sems.at[i])
-        for i, (src, dst) in enumerate(((gate_hbm, gate_ref), (up_hbm, up_ref), (down_hbm, down_ref)))
+        for i, (src, dst) in enumerate(
+            (
+                (route_hbm, route_ref),
+                (weight_hbm, weight_ref),
+                (gate_hbm, gate_ref),
+                (up_hbm, up_ref),
+                (down_hbm, down_ref),
+                (shared_gate_hbm, shared_gate_ref),
+                (shared_up_hbm, shared_up_ref),
+                (shared_down_hbm, shared_down_ref),
+            )
+        )
     ]
     for load in loads:
         load.start()
@@ -159,28 +167,44 @@
         ],
         axis=1,
     )
-    hidden = []
-    for own, (g, u) in enumerate(((gate2_ref, up2_ref), (gate_ref, up_ref))):
-        if own:
-            loads[0].wait()
-            loads[1].wait()
-        gate = jnp.dot(inputs, g[...], preferred_element_type=F32)
-        upward = jnp.dot(inputs, u[...], preferred_element_type=F32)
-        hidden.append((gate * jax.nn.sigmoid(gate) * upward).astype(BF16))
+
+    def swiglu(values, g, u):
+        gate = jnp.dot(values, g[...], preferred_element_type=F32)
+        upward = jnp.dot(values, u[...], preferred_element_type=F32)
+        return (gate * jax.nn.sigmoid(gate) * upward).astype(BF16)
+
+    hidden2 = swiglu(inputs, gate2_ref, up2_ref)
+    loads[2].wait()
+    loads[3].wait()
+    hidden = swiglu(inputs, gate_ref, up_ref)
     back = order.T
-    loads[2].wait()
+    loads[4].wait()
     results = []
     for q in range(pieces):
         span = slice(q * piece, (q + 1) * piece)
         results.append(
             (
-                jnp.dot(hidden[0], down2_ref[:, span], preferred_element_type=F32)
-                + jnp.dot(hidden[1], down_ref[:, span], preferred_element_type=F32)
+                jnp.dot(hidden2, down2_ref[:, span], preferred_element_type=F32)
+                + jnp.dot(hidden, down_ref[:, span], preferred_element_type=F32)
             ).astype(BF16)
         )
     for h in range(2):
         lined = jnp.concatenate([r[h * half : (h + 1) * half] for r in results], axis=0)
         out_ref[h * block : (h + 1) * block, :] = jnp.dot(back, lined, preferred_element_type=F32).astype(BF16)
+
+    for load in loads[:2] + loads[5:]:
+        load.wait()
+    normed = normed_ref[...]
+    tokens = normed.shape[0]
+    hidden = swiglu(normed, shared_gate_ref, shared_up_ref)
+    for q in range(pieces):
+        part_ref[q * tokens : (q + 1) * tokens, :] = jnp.dot(
+            hidden, shared_down_ref[:, q * piece : (q + 1) * piece], preferred_element_type=F32
+        )
+    mix = chosen(route_ref[...], core, slots, pieces, experts, weight_ref[...]).T
+    high = mix.astype(BF16)
+    mix_ref[: mix.shape[0], :] = high
+    mix_ref[mix.shape[0] :, :] = (mix - high.astype(F32)).astype(BF16)
 
 
 def combine_kernel(mix_ref, returned_ref, part_ref, out_ref):
@@ -252,27 +276,20 @@
     with jax.named_scope("outward"):
         arrived = lax.all_to_all(send.reshape(experts, slots * pieces, piece), "ep", 0, 0, tiled=True)
 
-    part, mix = pl.pallas_call(
-        functools.partial(shared_kernel, **sizes),
+    loaded = (*weights, shared_gate, shared_up, shared_down, route_expert.T, route_weight.T)
+    results, part, mix = pl.pallas_call(
+        functools.partial(expert_kernel, **sizes),
         out_shape=(
+            VMEM((rows, piece), BF16),
             VMEM((pieces * local_tokens, piece), F32),
             VMEM((2 * pieces * local_tokens, rows), BF16),
         ),
-        in_specs=[whole()] * 6,
-        out_specs=(whole(), whole()),
-        compiler_params=grant(8),
-        name="shared",
-    )(*held(normed, shared_gate, shared_up, shared_down, route_expert.T, route_weight.T))
-
-    results = pl.pallas_call(
-        functools.partial(expert_kernel, pieces=pieces),
-        out_shape=VMEM((rows, piece), BF16),
-        in_specs=[whole()] * 4 + [anywhere()] * 3,
-        out_specs=whole(),
-        scratch_shapes=[VMEM(w.shape, BF16) for w in weights] + [pltpu.SemaphoreType.DMA((3,))],
-        compiler_params=grant(12),
+        in_specs=[whole()] * 5 + [anywhere()] * len(loaded),
+        out_specs=(whole(),) * 3,
+        scratch_shapes=[VMEM(w.shape, w.dtype) for w in loaded] + [pltpu.SemaphoreType.DMA((len(loaded),))],
+        compiler_params=grant(20),
         name="expert",
-    )(*held(arrived.reshape(rows, piece), *others), *far(*weights))
+    )(*held(arrived.reshape(rows, piece), normed, *others), *far(*loaded))
     with jax.named_scope("homeward"):
         returned = lax.all_to_all(results.reshape(experts, slots * pieces, piece), "ep", 0, 0, tiled=True)
 

time: 80 us -> 80 us (level)
  blocking collectives: 22.4 us -> 45.8 us
  waiting for transfers between devices: 12.6 us -> 1.17 us
  starting transfers between devices: 32.8 us -> 24.8 us
  local copies, waits for them, and re-layouts: 2.83 us -> 0.01 us
  Pallas kernels: 8.95 us -> 8.02 us
    all_to_all x0 -> x1, blocking collectives: none -> 23.4 us  [body(): lax.all_to_all(results.reshape(experts, slots * pieces, piece), 'ep', 0,...]
    all_to_all x1 -> x0, waiting for transfers between devices: 11.4 us -> none  [body(): lax.all_to_all(results.reshape(experts, slots * pieces, piece), 'ep', 0,...]
    all_to_all x1 -> x0, starting transfers between devices: 8.04 us -> none  [body(): lax.all_to_all(results.reshape(experts, slots * pieces, piece), 'ep', 0,...]
    unnamed x12 -> x2, local copies, waits for them, and re-layouts: 2.83 us -> 0.01 us
    pallas_call x2 -> x1, Pallas kernels: 6.42 us -> 5.49 us  [body(): pl.pallas_call(functools.partial(expert_kernel, **sizes), out_shape=(VMEM...]
  transfers between devices with their start and end apart: 5 -> 4, of which waited for: 2 -> 1; matrix products, arithmetic and copies ran while one was open for 0% -> 0% of each run, Pallas kernels for 3% -> 2%
where the time goes in v3:
time: 80 us; the launch traced here: 79.8 us
  blocking collectives  45.8 us (57%)
  starting transfers between devices  24.8 us (31%)
  Pallas kernels  8.02 us (10%)
  waiting for transfers between devices  1.17 us (1%)
    all_to_all x1, blocking collectives, body(): lax.all_to_all(results.reshape(experts, slots * pieces, piece), 'ep', 0,...  23.4 us
    all_to_all x1, blocking collectives, body(): lax.all_to_all(send.reshape(experts, slots * pieces, piece), 'ep', 0, 0,...  22.4 us
    ppermute x3, starting transfers between devices, body(): others = tuple((lax.ppermute(w, 'tp', swap) for w in weights))  20.9 us
    pallas_call x1, Pallas kernels, body(): pl.pallas_call(functools.partial(expert_kernel, **sizes), out_shape=(VMEM...  5.49 us
    ppermute x1, starting transfers between devices, body(): other = lax.ppermute(mine, 'tp', swap)  3.88 us
  transfers between devices with their start and end apart: 4, of which 1 were waited for; matrix products, arithmetic and copies ran while one was open for 0% of the time, Pallas kernels for 2%

profile of v3, /device:TPU:513, one launch (start us, length us, event | category | flops | bytes accessed | tf_op | source)
XLA Modules:
  0.0 79.8 jit_solution(14900791310088174928)
XLA Ops:
  0.0 20.4 %collective-permute-start = (bf16[2048,384]{1,0:T(8,128)(2,1)}, bf16[2048,384]{1,0:T(8,128)(2,1)S(1)}, u32[]{:S(2)}, u32[]{:S(2)}) collective-permute-start(bf16[2048,384]{1,0:T(8,128)(2,1)} %bitcast.13), channel_id=1, source_target_pairs={{0,1},{1,0},{2,3},{3,2},{4,5},{5,4},{6,7},{7,6},{8,9},{9,8},{10,11... | collective-permute-start | bytes 4718600 | tf_op jit(solution)/shard_map/ppermute | solution.py:257
  20.4 0.0 collective-permute-start.1
  20.4 0.5 collective-permute-start.2
  20.9 1.5 %dispatch.1 = (bf16[512,512]{1,0:T(8,128)(2,1)S(1)}, bf16[32,2048]{1,0:T(8,128)(2,1)S(1)}) custom-call(bf16[32,2048]{1,0:T(8,128)(2,1)} %tokens_hbm.1, bf16[2048]{0:T(1024)(128)(2,1)} %gain_hbm.1, s32[6,32]{1,0:T(8,128)} %bitcast.19), custom_call_target="tpu_custom_call" | custom-call | tf_op jit(solution)/shard_map/dispatch/pallas_call | solution.py:259
  22.4 22.4 %all_to_all.10 = bf16[64,8,512]{2,1,0:T(8,128)(2,1)S(1)} all-to-all(bf16[64,8,512]{2,1,0:T(8,128)(2,1)S(1)} %bitcast.12), channel_id=1, replica_groups=mesh['grp'=2,'ep'=64,'tp'=2] {'ep'}, dimensions={0} | all-to-all | bytes 1048576 | tf_op jit(solution)/shard_map/outward/all_to_all | solution.py:277
  44.9 0.0 collective-permute-done.gate2_ref
  44.9 0.0 collective-permute-done.1.up2_ref
  44.9 0.0 collective-permute-done.2.down2_ref
  44.9 5.5 %expert.1 = (bf16[512,512]{1,0:T(8,128)(2,1)S(1)}, f32[128,512]{1,0:T(8,128)S(1)}, bf16[256,512]{1,0:T(8,128)(2,1)S(1)}) custom-call(bf16[512,512]{1,0:T(8,128)(2,1)S(1)} %bitcast.9, bf16[32,2048]{1,0:T(8,128)(2,1)S(1)} %get-tuple-element.11.normed_ref, bf16[2048,384]{1,0:T(8,128)(2,1)S(1)} %collective-permute-done.gate2_ref, ...), custom_call_target="tpu_custom_call" | custom-call | tf_op jit(solution)/shard_map/expert/pallas_call | solution.py:280
  50.4 0.0 copy-start
  50.4 23.4 %all_to_all.11 = bf16[64,8,512]{2,1,0:T(8,128)(2,1)S(1)} all-to-all(bf16[64,8,512]{2,1,0:T(8,128)(2,1)S(1)} %bitcast.11), channel_id=1, replica_groups=mesh['grp'=2,'ep'=64,'tp'=2] {'ep'}, dimensions={0} | all-to-all | bytes 1048576 | tf_op jit(solution)/shard_map/homeward/all_to_all | solution.py:294
  73.7 0.3 combine.1.mine_ref
  74.0 3.9 %collective-permute-start.3 = (f32[128,512]{1,0:T(8,128)S(1)}, f32[128,512]{1,0:T(8,128)S(1)}, u32[]{:S(2)}, u32[]{:S(2)}) collective-permute-start(f32[128,512]{1,0:T(8,128)S(1)} %combine.1.mine_ref), channel_id=1, source_target_pairs={{0,1},{1,0},{2,3},{3,2},{4,5},{5,4},{6,7},{7,6},{8,9},{9,8},{10,11... | collective-permute-start | bytes 786440 | tf_op jit(solution)/shard_map/ppermute | solution.py:304
  77.9 1.2 %collective-permute-done.3.other_ref = f32[128,512]{1,0:T(8,128)S(1)} collective-permute-done((f32[128,512]{1,0:T(8,128)S(1)}, f32[128,512]{1,0:T(8,128)S(1)}, u32[]{:S(2)}, u32[]{:S(2)}) %collective-permute-start.3) | collective-permute-done | bytes 262176 | tf_op jit(solution)/shard_map/ppermute | solution.py:304
  79.1 0.0 copy-done
  79.1 0.8 closing.1
Async XLA Ops:
  0.0 44.9 %collective-permute-start = (bf16[2048,384]{1,0:T(8,128)(2,1)}, bf16[2048,384]{1,0:T(8,128)(2,1)S(1)}, u32[]{:S(2)}, u32[]{:S(2)}) collective-permute-start(bf16[2048,384]{1,0:T(8,128)(2,1)} %bitcast.13), channel_id=1, source_target_pairs={{0,1},{1,0},{2,3},{3,2},{4,5},{5,4},{6,7},{7,6},{8,9},{9,8},{10,11... | collective-permute-start | bytes 4718600 | tf_op jit(solution)/shard_map/ppermute | solution.py:257
  20.4 24.4 %collective-permute-start.1 = (bf16[2048,384]{1,0:T(8,128)(2,1)}, bf16[2048,384]{1,0:T(8,128)(2,1)S(1)}, u32[]{:S(2)}, u32[]{:S(2)}) collective-permute-start(bf16[2048,384]{1,0:T(8,128)(2,1)} %bitcast.15), channel_id=1, source_target_pairs={{0,1},{1,0},{2,3},{3,2},{4,5},{5,4},{6,7},{7,6},{8,9},{9,8},{10,11... | collective-permute-start | bytes 4718600 | tf_op jit(solution)/shard_map/ppermute | solution.py:257
  20.4 24.4 %collective-permute-start.2 = (bf16[384,2048]{1,0:T(8,128)(2,1)}, bf16[384,2048]{1,0:T(8,128)(2,1)S(1)}, u32[]{:S(2)}, u32[]{:S(2)}) collective-permute-start(bf16[384,2048]{1,0:T(8,128)(2,1)} %bitcast.17), channel_id=1, source_target_pairs={{0,1},{1,0},{2,3},{3,2},{4,5},{5,4},{6,7},{7,6},{8,9},{9,8},{10,11... | collective-permute-start | bytes 4718600 | tf_op jit(solution)/shard_map/ppermute | solution.py:257
  50.4 28.7 %copy-start = (bf16[1024]{0:T(1024)(128)(2,1)S(1)}, bf16[1024]{0:T(1024)(128)(2,1)}, u32[]{:S(2)}) copy-start(bf16[1024]{0:T(1024)(128)(2,1)} %gain_ref.1) | copy-start | bytes 6148
  74.0 5.0 %collective-permute-start.3 = (f32[128,512]{1,0:T(8,128)S(1)}, f32[128,512]{1,0:T(8,128)S(1)}, u32[]{:S(2)}, u32[]{:S(2)}) collective-permute-start(f32[128,512]{1,0:T(8,128)S(1)} %combine.1.mine_ref), channel_id=1, source_target_pairs={{0,1},{1,0},{2,3},{3,2},{4,5},{5,4},{6,7},{7,6},{8,9},{9,8},{10,11... | collective-permute-start | bytes 786440 | tf_op jit(solution)/shard_map/ppermute | solution.py:304

commit v4 on v2

--- a/solution.py
+++ b/solution.py
@@ -6,6 +6,7 @@
 from jax.experimental import pallas as pl
 from jax.experimental.pallas import tpu as pltpu
 from jax.sharding import PartitionSpec as P
+
 
 EPSILON = 1e-06
 F32 = jnp.float32
@@ -97,50 +98,91 @@
     send_ref[...] = jnp.dot(pick, stacked, preferred_element_type=F32).astype(BF16)
 
 
-def shared_kernel(
-    normed_ref, gate_ref, up_ref, down_ref, route_ref, weight_ref, part_ref, mix_ref, *, slots, pieces, experts
+def gathering(half, pieces):
+    to, frm = iota((half * pieces, half * pieces), 0), iota((half * pieces, half * pieces), 1)
+    return jnp.where(frm == (to % half) * pieces + to // half, 1.0, 0.0).astype(BF16)
+
+
+def swiglu(values, g, u):
+    gate = jnp.dot(values, g[...], preferred_element_type=F32)
+    upward = jnp.dot(values, u[...], preferred_element_type=F32)
+    return (gate * jax.nn.sigmoid(gate) * upward).astype(BF16)
+
+
+def side_kernel(
+    normed_ref,
+    shared_gate_hbm,
+    shared_up_hbm,
+    shared_down_hbm,
+    route_hbm,
+    weight_hbm,
+    part_ref,
+    mix_ref,
+    shared_gate_ref,
+    shared_up_ref,
+    shared_down_ref,
+    route_ref,
+    weight_ref,
+    sems,
+    *,
+    slots,
+    pieces,
+    experts,
 ):
     core = lax.axis_index("tp")
-    normed = normed_ref[...]
-    gate = jnp.dot(normed, gate_ref[...], preferred_element_type=F32)
-    upward = jnp.dot(normed, up_ref[...], preferred_element_type=F32)
-    hidden = (gate * jax.nn.sigmoid(gate) * upward).astype(BF16)
-    tokens, piece = normed.shape[0], normed.shape[1] // pieces
-    for q in range(pieces):
-        part_ref[q * tokens : (q + 1) * tokens, :] = jnp.dot(
-            hidden, down_ref[:, q * piece : (q + 1) * piece], preferred_element_type=F32
-        )
+    pairs = (
+        (route_hbm, route_ref),
+        (weight_hbm, weight_ref),
+        (shared_gate_hbm, shared_gate_ref),
+        (shared_up_hbm, shared_up_ref),
+        (shared_down_hbm, shared_down_ref),
+    )
+    loads = [pltpu.make_async_copy(src, dst, sems.at[i]) for i, (src, dst) in enumerate(pairs)]
+    for load in loads:
+        load.start()
+    for load in loads[:2]:
+        load.wait()
     mix = chosen(route_ref[...], core, slots, pieces, experts, weight_ref[...]).T
     high = mix.astype(BF16)
     mix_ref[: mix.shape[0], :] = high
     mix_ref[mix.shape[0] :, :] = (mix - high.astype(F32)).astype(BF16)
-
-
-def gathering(half, pieces):
-    to, frm = iota((half * pieces, half * pieces), 0), iota((half * pieces, half * pieces), 1)
-    return jnp.where(frm == (to % half) * pieces + to // half, 1.0, 0.0).astype(BF16)
+    for load in loads[2:]:
+        load.wait()
+    normed = normed_ref[...]
+    tokens, piece = normed.shape[0], normed.shape[1] // pieces
+    hidden = swiglu(normed, shared_gate_ref, shared_up_ref)
+    for q in range(pieces):
+        part_ref[q * tokens : (q + 1) * tokens, :] = jnp.dot(
+            hidden, shared_down_ref[:, q * piece : (q + 1) * piece], preferred_element_type=F32
+        )
 
 
 def expert_kernel(
     rows_ref,
     gate2_ref,
-    up2_ref,
-    down2_ref,
+    up2_hbm,
     gate_hbm,
     up_hbm,
+    down2_hbm,
     down_hbm,
     out_ref,
+    up2_ref,
     gate_ref,
     up_ref,
+    down2_ref,
     down_ref,
     sems,
     *,
     pieces,
 ):
-    loads = [
-        pltpu.make_async_copy(src, dst, sems.at[i])
-        for i, (src, dst) in enumerate(((gate_hbm, gate_ref), (up_hbm, up_ref), (down_hbm, down_ref)))
-    ]
+    pairs = (
+        (up2_hbm, up2_ref),
+        (gate_hbm, gate_ref),
+        (up_hbm, up_ref),
+        (down2_hbm, down2_ref),
+        (down_hbm, down_ref),
+    )
+    loads = [pltpu.make_async_copy(src, dst, sems.at[i]) for i, (src, dst) in enumerate(pairs)]
     for load in loads:
         load.start()
     total = rows_ref.shape[0]
@@ -159,23 +201,21 @@
         ],
         axis=1,
     )
-    hidden = []
-    for own, (g, u) in enumerate(((gate2_ref, up2_ref), (gate_ref, up_ref))):
-        if own:
-            loads[0].wait()
-            loads[1].wait()
-        gate = jnp.dot(inputs, g[...], preferred_element_type=F32)
-        upward = jnp.dot(inputs, u[...], preferred_element_type=F32)
-        hidden.append((gate * jax.nn.sigmoid(gate) * upward).astype(BF16))
+    loads[0].wait()
+    hidden2 = swiglu(inputs, gate2_ref, up2_ref)
+    loads[1].wait()
+    loads[2].wait()
+    hidden = swiglu(inputs, gate_ref, up_ref)
+    loads[3].wait()
+    loads[4].wait()
     back = order.T
-    loads[2].wait()
     results = []
     for q in range(pieces):
         span = slice(q * piece, (q + 1) * piece)
         results.append(
             (
-                jnp.dot(hidden[0], down2_ref[:, span], preferred_element_type=F32)
-                + jnp.dot(hidden[1], down_ref[:, span], preferred_element_type=F32)
+                jnp.dot(hidden, down_ref[:, span], preferred_element_type=F32)
+                + jnp.dot(hidden2, down2_ref[:, span], preferred_element_type=F32)
             ).astype(BF16)
         )
     for h in range(2):
@@ -249,32 +289,33 @@
         compiler_params=grant(6),
         name="dispatch",
     )(*far(tokens, in_gain, route_expert.T))
-    with jax.named_scope("outward"):
-        arrived = lax.all_to_all(send.reshape(experts, slots * pieces, piece), "ep", 0, 0, tiled=True)
-
+    arrived = lax.all_to_all(send.reshape(experts, slots * pieces, piece), "ep", 0, 0, tiled=True)
+
+    loaded = (shared_gate, shared_up, shared_down, route_expert.T, route_weight.T)
     part, mix = pl.pallas_call(
-        functools.partial(shared_kernel, **sizes),
+        functools.partial(side_kernel, **sizes),
         out_shape=(
             VMEM((pieces * local_tokens, piece), F32),
             VMEM((2 * pieces * local_tokens, rows), BF16),
         ),
-        in_specs=[whole()] * 6,
+        in_specs=[whole()] + [anywhere()] * len(loaded),
         out_specs=(whole(), whole()),
-        compiler_params=grant(8),
-        name="shared",
-    )(*held(normed, shared_gate, shared_up, shared_down, route_expert.T, route_weight.T))
-
+        scratch_shapes=[VMEM(w.shape, w.dtype) for w in loaded] + [pltpu.SemaphoreType.DMA((len(loaded),))],
+        compiler_params=grant(12),
+        name="side",
+    )(*held(normed), *far(*loaded))
+
+    fetched = (others[1], weights[0], weights[1], others[2], weights[2])
     results = pl.pallas_call(
         functools.partial(expert_kernel, pieces=pieces),
         out_shape=VMEM((rows, piece), BF16),
-        in_specs=[whole()] * 4 + [anywhere()] * 3,
+        in_specs=[whole()] * 2 + [anywhere()] * len(fetched),
         out_specs=whole(),
-        scratch_shapes=[VMEM(w.shape, BF16) for w in weights] + [pltpu.SemaphoreType.DMA((3,))],
-        compiler_params=grant(12),
+        scratch_shapes=[VMEM(w.shape, w.dtype) for w in fetched] + [pltpu.SemaphoreType.DMA((len(fetched),))],
+        compiler_params=grant(16),
         name="expert",
-    )(*held(arrived.reshape(rows, piece), *others), *far(*weights))
-    with jax.named_scope("homeward"):
-        returned = lax.all_to_all(results.reshape(experts, slots * pieces, piece), "ep", 0, 0, tiled=True)
+    )(*held(arrived.reshape(rows, piece), others[0]), *far(*fetched))
+    returned = lax.all_to_all(results.reshape(experts, slots * pieces, piece), "ep", 0, 0, tiled=True)
 
     mine = pl.pallas_call(
         combine_kernel,

time: 80 us -> 81.6 us (1.020)
  Pallas kernels: 8.95 us -> 11.1 us
  local copies, waits for them, and re-layouts: 2.83 us -> 1.62 us
    pallas_call x1, Pallas kernels: 1.27 us -> 3.42 us  [body(): pl.pallas_call(functools.partial(side_kernel, **sizes), out_shape=(VMEM((...]
    unnamed x12 -> x6, local copies, waits for them, and re-layouts: 2.83 us -> 1.62 us
  transfers between devices with their start and end apart: 5 -> 5, of which waited for: 2 -> 2; matrix products, arithmetic and copies ran while one was open for 0% -> 0% of each run, Pallas kernels for 3% -> 6%
where the time goes in v4:
time: 81.6 us; the launch traced here: 81.4 us
  starting transfers between devices  32.8 us (40%)
  blocking collectives  22.4 us (27%)
  waiting for transfers between devices  13.3 us (16%)
  Pallas kernels  11.1 us (14%)
  local copies, waits for them, and re-layouts  1.62 us (2%)
    all_to_all x1, blocking collectives, body(): lax.all_to_all(send.reshape(experts, slots * pieces, piece), 'ep', 0, 0,...  22.4 us
    ppermute x3, starting transfers between devices, body(): others = tuple((lax.ppermute(w, 'tp', swap) for w in weights))  20.9 us
    all_to_all x1, waiting for transfers between devices, body(): lax.all_to_all(results.reshape(experts, slots * pieces, piece), 'ep', 0,...  12.1 us
    all_to_all x1, starting transfers between devices, body(): lax.all_to_all(results.reshape(experts, slots * pieces, piece), 'ep', 0,...  8.04 us
    pallas_call x1, Pallas kernels, body(): pl.pallas_call(functools.partial(expert_kernel, pieces=pieces), out_shape...  5.19 us
    ppermute x1, starting transfers between devices, body(): other = lax.ppermute(mine, 'tp', swap)  3.88 us
    pallas_call x1, Pallas kernels, body(): pl.pallas_call(functools.partial(side_kernel, **sizes), out_shape=(VMEM((...  3.42 us
  transfers between devices with their start and end apart: 5, of which 2 were waited for; matrix products, arithmetic and copies ran while one was open for 0% of the time, Pallas kernels for 6%

profile of v4, /device:TPU:513, one launch (start us, length us, event | category | flops | bytes accessed | tf_op | source)
XLA Modules:
  0.0 81.4 jit_solution(2845190676993253448)
XLA Ops:
  0.0 20.4 %collective-permute-start = (bf16[2048,384]{1,0:T(8,128)(2,1)}, bf16[2048,384]{1,0:T(8,128)(2,1)S(1)}, u32[]{:S(2)}, u32[]{:S(2)}) collective-permute-start(bf16[2048,384]{1,0:T(8,128)(2,1)} %bitcast.12), channel_id=1, source_target_pairs={{0,1},{1,0},{2,3},{3,2},{4,5},{5,4},{6,7},{7,6},{8,9},{9,8},{10,11... | collective-permute-start | bytes 4718600 | tf_op jit(solution)/shard_map/ppermute | solution.py:273
  20.4 0.0 collective-permute-start.1
  20.4 0.5 collective-permute-start.2
  20.9 1.5 %dispatch.1 = (bf16[512,512]{1,0:T(8,128)(2,1)S(1)}, bf16[32,2048]{1,0:T(8,128)(2,1)S(1)}) custom-call(bf16[32,2048]{1,0:T(8,128)(2,1)} %tokens_hbm.1, bf16[2048]{0:T(1024)(128)(2,1)} %gain_hbm.1, s32[6,32]{1,0:T(8,128)} %bitcast.18), custom_call_target="tpu_custom_call" | custom-call | tf_op jit(solution)/shard_map/dispatch/pallas_call | solution.py:275
  22.4 22.4 %all_to_all.10 = bf16[64,8,512]{2,1,0:T(8,128)(2,1)S(1)} all-to-all(bf16[64,8,512]{2,1,0:T(8,128)(2,1)S(1)} %bitcast.11), channel_id=1, replica_groups=mesh['grp'=2,'ep'=64,'tp'=2] {'ep'}, dimensions={0} | all-to-all | bytes 1048576 | tf_op jit(solution)/shard_map/all_to_all | solution.py:292
  44.9 0.0 collective-permute-done.gate2_ref
  44.9 0.0 collective-permute-done.1.up2_hbm
  44.9 0.0 copy-start.1
  44.9 0.0 collective-permute-done.2.down2_hbm
  44.9 0.0 copy-start.2
  44.9 1.1 %copy-done.1 = bf16[2048,384]{1,0:T(8,128)(2,1)} copy-done((bf16[2048,384]{1,0:T(8,128)(2,1)}, bf16[2048,384]{1,0:T(8,128)(2,1)S(1)}, u32[]{:S(2)}) %copy-start.1) | copy-done | bytes 1572888
  46.0 0.5 copy-done.2
  46.5 5.2 %expert.1 = bf16[512,512]{1,0:T(8,128)(2,1)} custom-call(bf16[512,512]{1,0:T(8,128)(2,1)S(1)} %bitcast.9, bf16[2048,384]{1,0:T(8,128)(2,1)S(1)} %collective-permute-done.gate2_ref, bf16[2048,384]{1,0:T(8,128)(2,1)} %copy-done.1, bf16[2048,384]{1,0:T(8,128)(2,1)} %bitcast.13, bf16[2048,384]{1,0:T(8,128)(2,1)} %bitcast.15, bf16[384,2048]{1,0:T(8,128)(2,1)} %copy-done.2, ...), custom_call_target="tpu_custom_call" | custom-call | tf_op jit(solution)/shard_map/expert/pallas_call | solution.py:309
  51.7 8.0 %all-to-all-start.1 = ((bf16[64,8,512]{2,1,0:T(8,128)(2,1)}), bf16[64,8,512]{2,1,0:T(8,128)(2,1)S(1)}, u32[]{:S(2)}, u32[]{:S(2)}) async-start(bf16[64,8,512]{2,1,0:T(8,128)(2,1)} %bitcast.7), calls=%async_computation.1 | async-start | bytes 1048576 | tf_op jit(solution)/shard_map/all_to_all | solution.py:318
  59.7 0.0 copy-start
  59.7 3.4 %side.1 = (f32[128,512]{1,0:T(8,128)S(1)}, bf16[256,512]{1,0:T(8,128)(2,1)S(1)}) custom-call(bf16[32,2048]{1,0:T(8,128)(2,1)S(1)} %get-tuple-element.9.normed_ref, bf16[2048,384]{1,0:T(8,128)(2,1)} %shared_gate_hbm.1, bf16[2048,384]{1,0:T(8,128)(2,1)} %shared_up_hbm.1, bf16[384,2048]{1,0:T(8,128)(2,1)} %shared_down_hbm.1, s32[6,32]{1,0:T(8,128)} %bitcast.19, ...), custom_call_target="tpu_custom_call" | custom-call | tf_op jit(solution)/shard_map/side/pallas_call | solution.py:295
  63.2 12.1 %all-to-all-done.1 = bf16[64,8,512]{2,1,0:T(8,128)(2,1)S(1)} async-done(((bf16[64,8,512]{2,1,0:T(8,128)(2,1)}), bf16[64,8,512]{2,1,0:T(8,128)(2,1)S(1)}, u32[]{:S(2)}, u32[]{:S(2)}) %all-to-all-start.1) | async-done | bytes 524320 | tf_op jit(solution)/shard_map/all_to_all | solution.py:318
  75.3 0.3 combine.1.mine_ref
  75.6 3.9 %collective-permute-start.3 = (f32[128,512]{1,0:T(8,128)S(1)}, f32[128,512]{1,0:T(8,128)S(1)}, u32[]{:S(2)}, u32[]{:S(2)}) collective-permute-start(f32[128,512]{1,0:T(8,128)S(1)} %combine.1.mine_ref), channel_id=1, source_target_pairs={{0,1},{1,0},{2,3},{3,2},{4,5},{5,4},{6,7},{7,6},{8,9},{9,8},{10,11... | collective-permute-start | bytes 786440 | tf_op jit(solution)/shard_map/ppermute | solution.py:328
  79.4 1.2 %collective-permute-done.3.other_ref = f32[128,512]{1,0:T(8,128)S(1)} collective-permute-done((f32[128,512]{1,0:T(8,128)S(1)}, f32[128,512]{1,0:T(8,128)S(1)}, u32[]{:S(2)}, u32[]{:S(2)}) %collective-permute-start.3) | collective-permute-done | bytes 262176 | tf_op jit(solution)/shard_map/ppermute | solution.py:328
  80.6 0.0 copy-done
  80.6 0.8 closing.1
Async XLA Ops:
  0.0 44.9 %collective-permute-start = (bf16[2048,384]{1,0:T(8,128)(2,1)}, bf16[2048,384]{1,0:T(8,128)(2,1)S(1)}, u32[]{:S(2)}, u32[]{:S(2)}) collective-permute-start(bf16[2048,384]{1,0:T(8,128)(2,1)} %bitcast.12), channel_id=1, source_target_pairs={{0,1},{1,0},{2,3},{3,2},{4,5},{5,4},{6,7},{7,6},{8,9},{9,8},{10,11... | collective-permute-start | bytes 4718600 | tf_op jit(solution)/shard_map/ppermute | solution.py:273
  20.4 24.4 %collective-permute-start.1 = (bf16[2048,384]{1,0:T(8,128)(2,1)}, bf16[2048,384]{1,0:T(8,128)(2,1)S(1)}, u32[]{:S(2)}, u32[]{:S(2)}) collective-permute-start(bf16[2048,384]{1,0:T(8,128)(2,1)} %bitcast.14), channel_id=1, source_target_pairs={{0,1},{1,0},{2,3},{3,2},{4,5},{5,4},{6,7},{7,6},{8,9},{9,8},{10,11... | collective-permute-start | bytes 4718600 | tf_op jit(solution)/shard_map/ppermute | solution.py:273
  20.4 24.5 %collective-permute-start.2 = (bf16[384,2048]{1,0:T(8,128)(2,1)}, bf16[384,2048]{1,0:T(8,128)(2,1)S(1)}, u32[]{:S(2)}, u32[]{:S(2)}) collective-permute-start(bf16[384,2048]{1,0:T(8,128)(2,1)} %bitcast.16), channel_id=1, source_target_pairs={{0,1},{1,0},{2,3},{3,2},{4,5},{5,4},{6,7},{7,6},{8,9},{9,8},{10,11... | collective-permute-start | bytes 4718600 | tf_op jit(solution)/shard_map/ppermute | solution.py:273
  44.9 1.2 %copy-start.1 = (bf16[2048,384]{1,0:T(8,128)(2,1)}, bf16[2048,384]{1,0:T(8,128)(2,1)S(1)}, u32[]{:S(2)}) copy-start(bf16[2048,384]{1,0:T(8,128)(2,1)S(1)} %collective-permute-done.1.up2_hbm) | copy-start | bytes 4718596
  44.9 1.6 %copy-start.2 = (bf16[384,2048]{1,0:T(8,128)(2,1)}, bf16[384,2048]{1,0:T(8,128)(2,1)S(1)}, u32[]{:S(2)}) copy-start(bf16[384,2048]{1,0:T(8,128)(2,1)S(1)} %collective-permute-done.2.down2_hbm) | copy-start | bytes 4718596
  51.7 23.6 %all-to-all-start.1 = ((bf16[64,8,512]{2,1,0:T(8,128)(2,1)}), bf16[64,8,512]{2,1,0:T(8,128)(2,1)S(1)}, u32[]{:S(2)}, u32[]{:S(2)}) async-start(bf16[64,8,512]{2,1,0:T(8,128)(2,1)} %bitcast.7), calls=%async_computation.1 | async-start | bytes 1048576 | tf_op jit(solution)/shard_map/all_to_all | solution.py:318
  59.7 20.9 %copy-start = (bf16[1024]{0:T(1024)(128)(2,1)S(1)}, bf16[1024]{0:T(1024)(128)(2,1)}, u32[]{:S(2)}) copy-start(bf16[1024]{0:T(1024)(128)(2,1)} %gain_ref.1) | copy-start | bytes 6148
  75.6 5.0 %collective-permute-start.3 = (f32[128,512]{1,0:T(8,128)S(1)}, f32[128,512]{1,0:T(8,128)S(1)}, u32[]{:S(2)}, u32[]{:S(2)}) collective-permute-start(f32[128,512]{1,0:T(8,128)S(1)} %combine.1.mine_ref), channel_id=1, source_target_pairs={{0,1},{1,0},{2,3},{3,2},{4,5},{5,4},{6,7},{7,6},{8,9},{9,8},{10,11... | collective-permute-start | bytes 786440 | tf_op jit(solution)/shard_map/ppermute | solution.py:328

commit v5 on v4

--- a/solution.py
+++ b/solution.py
@@ -1,4 +1,5 @@
 import functools
+import math
 
 import jax
 import jax.numpy as jnp
@@ -38,11 +39,22 @@
     return lax.broadcasted_iota(jnp.int32, shape, dim)
 
 
+def seated(block, experts):
+    side = math.isqrt(experts)
+    if side * side != experts or side % 2:
+        return block
+
+    def spread(i):
+        return i // 2 + i % 2 * (side // 2)
+
+    return experts - 1 - spread(block // side) * side - spread(block % side)
+
+
 def chosen(route, core, slots, pieces, experts, values=None):
     top, tokens = route.shape
     rows, lanes = experts * slots * pieces, pieces * tokens
     row, lane = iota((rows, lanes), 0), iota((rows, lanes), 1)
-    expert = row // (slots * pieces)
+    expert = seated(row // (slots * pieces), experts)
     tiled = jnp.concatenate([route] * pieces, axis=1)
     hits = [tiled[k : k + 1] == expert for k in range(top)]
     named = functools.reduce(jnp.logical_or, hits)
@@ -268,6 +280,10 @@
     rows = experts * slots * pieces
     sizes = dict(slots=slots, pieces=pieces, experts=experts)
 
+    order = [[seated(block, experts) for block in range(experts)]]
+    exchange = functools.partial(
+        lax.all_to_all, axis_name="ep", split_axis=0, concat_axis=0, axis_index_groups=order, tiled=True
+    )
     swap = [(i, (i + 1) % cores) for i in range(cores)]
     weights = (gate_weight[0], up_weight[0], down_weight[0])
     others = tuple(lax.ppermute(w, "tp", swap) for w in weights)
@@ -289,7 +305,7 @@
         compiler_params=grant(6),
         name="dispatch",
     )(*far(tokens, in_gain, route_expert.T))
-    arrived = lax.all_to_all(send.reshape(experts, slots * pieces, piece), "ep", 0, 0, tiled=True)
+    arrived = exchange(send.reshape(experts, slots * pieces, piece))
 
     loaded = (shared_gate, shared_up, shared_down, route_expert.T, route_weight.T)
     part, mix = pl.pallas_call(
@@ -315,7 +331,7 @@
         compiler_params=grant(16),
         name="expert",
     )(*held(arrived.reshape(rows, piece), others[0]), *far(*fetched))
-    returned = lax.all_to_all(results.reshape(experts, slots * pieces, piece), "ep", 0, 0, tiled=True)
+    returned = exchange(results.reshape(experts, slots * pieces, piece))
 
     mine = pl.pallas_call(
         combine_kernel,

time: 81.6 us -> 80.8 us (level)
  starting transfers between devices: 32.8 us -> 36 us
  waiting for transfers between devices: 13.3 us -> 10.1 us
  blocking collectives: 22.4 us -> 21.5 us
    all_to_all x1, starting transfers between devices: 8.04 us -> 12.1 us  [body(): returned = exchange(results.reshape(experts, slots * pieces, piece))]
    all_to_all x1, waiting for transfers between devices: 12.1 us -> 8.93 us  [body(): returned = exchange(results.reshape(experts, slots * pieces, piece))]
    all_to_all x1, blocking collectives: 22.4 us -> 21.5 us  [body(): arrived = exchange(send.reshape(experts, slots * pieces, piece))]
    ppermute x1, starting transfers between devices: 3.88 us -> 3 us  [body(): other = lax.ppermute(mine, 'tp', swap)]
where the time goes in v5:
time: 80.8 us; the launch traced here: 80.5 us
  starting transfers between devices  36 us (45%)
  blocking collectives  21.5 us (27%)
  Pallas kernels  11.2 us (14%)
  waiting for transfers between devices  10.1 us (12%)
  local copies, waits for them, and re-layouts  1.62 us (2%)
    all_to_all x1, blocking collectives, body(): arrived = exchange(send.reshape(experts, slots * pieces, piece))  21.5 us
    ppermute x3, starting transfers between devices, body(): others = tuple((lax.ppermute(w, 'tp', swap) for w in weights))  20.9 us
    all_to_all x1, starting transfers between devices, body(): returned = exchange(results.reshape(experts, slots * pieces, piece))  12.1 us
    all_to_all x1, waiting for transfers between devices, body(): returned = exchange(results.reshape(experts, slots * pieces, piece))  8.93 us
    pallas_call x1, Pallas kernels, body(): pl.pallas_call(functools.partial(expert_kernel, pieces=pieces), out_shape...  5.19 us
    pallas_call x1, Pallas kernels, body(): pl.pallas_call(functools.partial(side_kernel, **sizes), out_shape=(VMEM((...  3.42 us
    ppermute x1, starting transfers between devices, body(): other = lax.ppermute(mine, 'tp', swap)  3 us
    unnamed x6, local copies, waits for them, and re-layouts  1.62 us
  transfers between devices with their start and end apart: 5, of which 2 were waited for; matrix products, arithmetic and copies ran while one was open for 0% of the time, Pallas kernels for 6%

profile of v5, /device:TPU:513, one launch (start us, length us, event | category | flops | bytes accessed | tf_op | source)
XLA Modules:
  0.0 80.5 jit_solution(17512680418868438016)
XLA Ops:
  0.0 20.4 %collective-permute-start = (bf16[2048,384]{1,0:T(8,128)(2,1)}, bf16[2048,384]{1,0:T(8,128)(2,1)S(1)}, u32[]{:S(2)}, u32[]{:S(2)}) collective-permute-start(bf16[2048,384]{1,0:T(8,128)(2,1)} %bitcast.12), channel_id=1, source_target_pairs={{0,1},{1,0},{2,3},{3,2},{4,5},{5,4},{6,7},{7,6},{8,9},{9,8},{10,11... | collective-permute-start | bytes 4718600 | tf_op jit(solution)/shard_map/ppermute | solution.py:289
  20.4 0.0 collective-permute-start.1
  20.4 0.5 collective-permute-start.2
  20.9 1.6 %dispatch.1 = (bf16[512,512]{1,0:T(8,128)(2,1)S(1)}, bf16[32,2048]{1,0:T(8,128)(2,1)S(1)}) custom-call(bf16[32,2048]{1,0:T(8,128)(2,1)} %tokens_hbm.1, bf16[2048]{0:T(1024)(128)(2,1)} %gain_hbm.1, s32[6,32]{1,0:T(8,128)} %bitcast.18), custom_call_target="tpu_custom_call" | custom-call | tf_op jit(solution)/shard_map/dispatch/pallas_call | solution.py:291
  22.5 21.5 %all_to_all.10 = bf16[64,8,512]{2,1,0:T(8,128)(2,1)S(1)} all-to-all(bf16[64,8,512]{2,1,0:T(8,128)(2,1)S(1)} %bitcast.11), channel_id=1, replica_groups={{126,118,124,116,122,114,120,112,62,54,60,52,58,50,56,48,110,102,108,10..., dimensions={0} | all-to-all | bytes 1048576 | tf_op jit(solution)/shard_map/all_to_all | solution.py:308
  44.0 0.0 collective-permute-done.gate2_ref
  44.0 0.0 collective-permute-done.1.up2_hbm
  44.0 0.0 copy-start.1
  44.0 0.0 collective-permute-done.2.down2_hbm
  44.0 0.0 copy-start.2
  44.0 1.1 %copy-done.1 = bf16[2048,384]{1,0:T(8,128)(2,1)} copy-done((bf16[2048,384]{1,0:T(8,128)(2,1)}, bf16[2048,384]{1,0:T(8,128)(2,1)S(1)}, u32[]{:S(2)}) %copy-start.1) | copy-done | bytes 1572888
  45.2 0.5 copy-done.2
  45.7 5.2 %expert.1 = bf16[512,512]{1,0:T(8,128)(2,1)} custom-call(bf16[512,512]{1,0:T(8,128)(2,1)S(1)} %bitcast.9, bf16[2048,384]{1,0:T(8,128)(2,1)S(1)} %collective-permute-done.gate2_ref, bf16[2048,384]{1,0:T(8,128)(2,1)} %copy-done.1, bf16[2048,384]{1,0:T(8,128)(2,1)} %bitcast.13, bf16[2048,384]{1,0:T(8,128)(2,1)} %bitcast.15, bf16[384,2048]{1,0:T(8,128)(2,1)} %copy-done.2, ...), custom_call_target="tpu_custom_call" | custom-call | tf_op jit(solution)/shard_map/expert/pallas_call | solution.py:325
  50.8 12.1 %all-to-all-start.1 = ((bf16[64,8,512]{2,1,0:T(8,128)(2,1)}), bf16[64,8,512]{2,1,0:T(8,128)(2,1)S(1)}, u32[]{:S(2)}, u32[]{:S(2)}) async-start(bf16[64,8,512]{2,1,0:T(8,128)(2,1)} %bitcast.7), calls=%async_computation.1 | async-start | bytes 1048576 | tf_op jit(solution)/shard_map/all_to_all | solution.py:334
  62.9 0.0 copy-start
  62.9 3.4 %side.1 = (f32[128,512]{1,0:T(8,128)S(1)}, bf16[256,512]{1,0:T(8,128)(2,1)S(1)}) custom-call(bf16[32,2048]{1,0:T(8,128)(2,1)S(1)} %get-tuple-element.9.normed_ref, bf16[2048,384]{1,0:T(8,128)(2,1)} %shared_gate_hbm.1, bf16[2048,384]{1,0:T(8,128)(2,1)} %shared_up_hbm.1, bf16[384,2048]{1,0:T(8,128)(2,1)} %shared_down_hbm.1, s32[6,32]{1,0:T(8,128)} %bitcast.19, ...), custom_call_target="tpu_custom_call" | custom-call | tf_op jit(solution)/shard_map/side/pallas_call | solution.py:311
  66.4 8.9 %all-to-all-done.1 = bf16[64,8,512]{2,1,0:T(8,128)(2,1)S(1)} async-done(((bf16[64,8,512]{2,1,0:T(8,128)(2,1)}), bf16[64,8,512]{2,1,0:T(8,128)(2,1)S(1)}, u32[]{:S(2)}, u32[]{:S(2)}) %all-to-all-start.1) | async-done | bytes 524320 | tf_op jit(solution)/shard_map/all_to_all | solution.py:334
  75.3 0.3 combine.1.mine_ref
  75.6 3.0 %collective-permute-start.3 = (f32[128,512]{1,0:T(8,128)S(1)}, f32[128,512]{1,0:T(8,128)S(1)}, u32[]{:S(2)}, u32[]{:S(2)}) collective-permute-start(f32[128,512]{1,0:T(8,128)S(1)} %combine.1.mine_ref), channel_id=1, source_target_pairs={{0,1},{1,0},{2,3},{3,2},{4,5},{5,4},{6,7},{7,6},{8,9},{9,8},{10,11... | collective-permute-start | bytes 786440 | tf_op jit(solution)/shard_map/ppermute | solution.py:344
  78.6 1.2 %collective-permute-done.3.other_ref = f32[128,512]{1,0:T(8,128)S(1)} collective-permute-done((f32[128,512]{1,0:T(8,128)S(1)}, f32[128,512]{1,0:T(8,128)S(1)}, u32[]{:S(2)}, u32[]{:S(2)}) %collective-permute-start.3) | collective-permute-done | bytes 262176 | tf_op jit(solution)/shard_map/ppermute | solution.py:344
  79.8 0.0 copy-done
  79.8 0.8 closing.1
Async XLA Ops:
  0.0 44.0 %collective-permute-start = (bf16[2048,384]{1,0:T(8,128)(2,1)}, bf16[2048,384]{1,0:T(8,128)(2,1)S(1)}, u32[]{:S(2)}, u32[]{:S(2)}) collective-permute-start(bf16[2048,384]{1,0:T(8,128)(2,1)} %bitcast.12), channel_id=1, source_target_pairs={{0,1},{1,0},{2,3},{3,2},{4,5},{5,4},{6,7},{7,6},{8,9},{9,8},{10,11... | collective-permute-start | bytes 4718600 | tf_op jit(solution)/shard_map/ppermute | solution.py:289
  20.4 23.6 %collective-permute-start.1 = (bf16[2048,384]{1,0:T(8,128)(2,1)}, bf16[2048,384]{1,0:T(8,128)(2,1)S(1)}, u32[]{:S(2)}, u32[]{:S(2)}) collective-permute-start(bf16[2048,384]{1,0:T(8,128)(2,1)} %bitcast.14), channel_id=1, source_target_pairs={{0,1},{1,0},{2,3},{3,2},{4,5},{5,4},{6,7},{7,6},{8,9},{9,8},{10,11... | collective-permute-start | bytes 4718600 | tf_op jit(solution)/shard_map/ppermute | solution.py:289
  20.4 23.6 %collective-permute-start.2 = (bf16[384,2048]{1,0:T(8,128)(2,1)}, bf16[384,2048]{1,0:T(8,128)(2,1)S(1)}, u32[]{:S(2)}, u32[]{:S(2)}) collective-permute-start(bf16[384,2048]{1,0:T(8,128)(2,1)} %bitcast.16), channel_id=1, source_target_pairs={{0,1},{1,0},{2,3},{3,2},{4,5},{5,4},{6,7},{7,6},{8,9},{9,8},{10,11... | collective-permute-start | bytes 4718600 | tf_op jit(solution)/shard_map/ppermute | solution.py:289
  44.0 1.2 %copy-start.1 = (bf16[2048,384]{1,0:T(8,128)(2,1)}, bf16[2048,384]{1,0:T(8,128)(2,1)S(1)}, u32[]{:S(2)}) copy-start(bf16[2048,384]{1,0:T(8,128)(2,1)S(1)} %collective-permute-done.1.up2_hbm) | copy-start | bytes 4718596
  44.0 1.6 %copy-start.2 = (bf16[384,2048]{1,0:T(8,128)(2,1)}, bf16[384,2048]{1,0:T(8,128)(2,1)S(1)}, u32[]{:S(2)}) copy-start(bf16[384,2048]{1,0:T(8,128)(2,1)S(1)} %collective-permute-done.2.down2_hbm) | copy-start | bytes 4718596
  50.8 24.5 %all-to-all-start.1 = ((bf16[64,8,512]{2,1,0:T(8,128)(2,1)}), bf16[64,8,512]{2,1,0:T(8,128)(2,1)S(1)}, u32[]{:S(2)}, u32[]{:S(2)}) async-start(bf16[64,8,512]{2,1,0:T(8,128)(2,1)} %bitcast.7), calls=%async_computation.1 | async-start | bytes 1048576 | tf_op jit(solution)/shard_map/all_to_all | solution.py:334
  62.9 16.8 %copy-start = (bf16[1024]{0:T(1024)(128)(2,1)S(1)}, bf16[1024]{0:T(1024)(128)(2,1)}, u32[]{:S(2)}) copy-start(bf16[1024]{0:T(1024)(128)(2,1)} %gain_ref.1) | copy-start | bytes 6148
  75.6 4.2 %collective-permute-start.3 = (f32[128,512]{1,0:T(8,128)S(1)}, f32[128,512]{1,0:T(8,128)S(1)}, u32[]{:S(2)}, u32[]{:S(2)}) collective-permute-start(f32[128,512]{1,0:T(8,128)S(1)} %combine.1.mine_ref), channel_id=1, source_target_pairs={{0,1},{1,0},{2,3},{3,2},{4,5},{5,4},{6,7},{7,6},{8,9},{9,8},{10,11... | collective-permute-start | bytes 786440 | tf_op jit(solution)/shard_map/ppermute | solution.py:344

commit v6 on v5

--- a/solution.py
+++ b/solution.py
@@ -77,12 +77,14 @@
     tokens_hbm,
     gain_hbm,
     route_hbm,
-    send_ref,
+    send_hbm,
     normed_ref,
     tokens_ref,
     gain_ref,
     route_ref,
+    send_ref,
     sems,
+    out_sems,
     *,
     slots,
     pieces,
@@ -107,7 +109,19 @@
     normed_ref[...] = normed
     piece = normed.shape[1] // pieces
     stacked = jnp.concatenate([normed[:, q * piece : (q + 1) * piece] for q in range(pieces)], axis=0)
-    send_ref[...] = jnp.dot(pick, stacked, preferred_element_type=F32).astype(BF16)
+    chunk = send_ref.shape[0] // 4
+    stores = []
+    for c in range(4):
+        span = slice(c * chunk, (c + 1) * chunk)
+        send_ref[span, :] = jnp.dot(pick[span], stacked, preferred_element_type=F32).astype(BF16)
+        stores.append(
+            pltpu.make_async_copy(
+                send_ref.at[pl.ds(c * chunk, chunk)], send_hbm.at[pl.ds(c * chunk, chunk)], out_sems.at[c]
+            )
+        )
+        stores[-1].start()
+    for store in stores:
+        store.wait()
 
 
 def gathering(half, pieces):
@@ -169,65 +183,64 @@
         )
 
 
+def opening_kernel(
+    rows_ref, gate_hbm, up_hbm, down_hbm, inputs_ref, hidden_ref, down_ref, gate_ref, up_ref, sems, *, pieces
+):
+    pairs = ((gate_hbm, gate_ref), (up_hbm, up_ref), (down_hbm, down_ref))
+    loads = [pltpu.make_async_copy(src, dst, sems.at[i]) for i, (src, dst) in enumerate(pairs)]
+    for load in loads:
+        load.start()
+    total = rows_ref.shape[0]
+    block, half = total // 2, total // pieces // 2
+    piece = rows_ref.shape[1]
+    order = gathering(half, pieces)
+    for h in range(2):
+        part = jnp.dot(order, rows_ref[h * block : (h + 1) * block, :], preferred_element_type=F32).astype(BF16)
+        for q in range(pieces):
+            inputs_ref[h * half : (h + 1) * half, q * piece : (q + 1) * piece] = part[q * half : (q + 1) * half]
+    inputs = inputs_ref[...]
+    loads[0].wait()
+    gate = jnp.dot(inputs, gate_ref[...], preferred_element_type=F32)
+    loads[1].wait()
+    upward = jnp.dot(inputs, up_ref[...], preferred_element_type=F32)
+    hidden_ref[...] = (gate * jax.nn.sigmoid(gate) * upward).astype(BF16)
+    loads[2].wait()
+
+
 def expert_kernel(
-    rows_ref,
+    inputs_ref,
+    hidden_ref,
+    down_ref,
     gate2_ref,
     up2_hbm,
-    gate_hbm,
-    up_hbm,
     down2_hbm,
-    down_hbm,
     out_ref,
     up2_ref,
-    gate_ref,
-    up_ref,
     down2_ref,
-    down_ref,
     sems,
     *,
     pieces,
 ):
-    pairs = (
-        (up2_hbm, up2_ref),
-        (gate_hbm, gate_ref),
-        (up_hbm, up_ref),
-        (down2_hbm, down2_ref),
-        (down_hbm, down_ref),
-    )
+    pairs = ((up2_hbm, up2_ref), (down2_hbm, down2_ref))
     loads = [pltpu.make_async_copy(src, dst, sems.at[i]) for i, (src, dst) in enumerate(pairs)]
     for load in loads:
         load.start()
-    total = rows_ref.shape[0]
-    rows, block = total // pieces, total // 2
-    half = rows // 2
-    piece = rows_ref.shape[1]
-    order = gathering(half, pieces)
-    parts = [
-        jnp.dot(order, rows_ref[h * block : (h + 1) * block, :], preferred_element_type=F32).astype(BF16)
-        for h in range(2)
-    ]
-    inputs = jnp.concatenate(
-        [
-            jnp.concatenate([parts[h][q * half : (q + 1) * half] for h in range(2)], axis=0)
-            for q in range(pieces)
-        ],
-        axis=1,
-    )
+    total, piece = out_ref.shape
+    block, half = total // 2, total // pieces // 2
+    inputs = inputs_ref[...]
+    gate = jnp.dot(inputs, gate2_ref[...], preferred_element_type=F32)
+    firsts = jnp.dot(hidden_ref[...], down_ref[...], preferred_element_type=F32)
+    back = gathering(half, pieces).T
     loads[0].wait()
-    hidden2 = swiglu(inputs, gate2_ref, up2_ref)
+    upward = jnp.dot(inputs, up2_ref[...], preferred_element_type=F32)
+    hidden2 = (gate * jax.nn.sigmoid(gate) * upward).astype(BF16)
     loads[1].wait()
-    loads[2].wait()
-    hidden = swiglu(inputs, gate_ref, up_ref)
-    loads[3].wait()
-    loads[4].wait()
-    back = order.T
     results = []
     for q in range(pieces):
         span = slice(q * piece, (q + 1) * piece)
         results.append(
             (
-                jnp.dot(hidden, down_ref[:, span], preferred_element_type=F32)
-                + jnp.dot(hidden2, down2_ref[:, span], preferred_element_type=F32)
+                firsts[:, span] + jnp.dot(hidden2, down2_ref[:, span], preferred_element_type=F32)
             ).astype(BF16)
         )
     for h in range(2):
@@ -291,16 +304,18 @@
     send, normed = pl.pallas_call(
         functools.partial(dispatch_kernel, **sizes),
         out_shape=(
-            VMEM((rows, piece), BF16),
+            pltpu.HBM((rows, piece), BF16),
             VMEM((local_tokens, width), BF16),
         ),
         in_specs=[anywhere()] * 3,
-        out_specs=(whole(), whole()),
+        out_specs=(anywhere(), whole()),
         scratch_shapes=[
             VMEM(tokens.shape, BF16),
             VMEM(in_gain.shape, BF16),
             VMEM(route_expert.shape[::-1], jnp.int32),
+            VMEM((rows, piece), BF16),
             pltpu.SemaphoreType.DMA((3,)),
+            pltpu.SemaphoreType.DMA((4,)),
         ],
         compiler_params=grant(6),
         name="dispatch",
@@ -321,16 +336,30 @@
         name="side",
     )(*held(normed), *far(*loaded))
 
-    fetched = (others[1], weights[0], weights[1], others[2], weights[2])
+    inputs, hidden, down = pl.pallas_call(
+        functools.partial(opening_kernel, pieces=pieces),
+        out_shape=(
+            VMEM((rows // pieces, width), BF16),
+            VMEM((rows // pieces, weights[0].shape[1]), BF16),
+            VMEM(weights[2].shape, BF16),
+        ),
+        in_specs=[whole()] + [anywhere()] * 3,
+        out_specs=(whole(),) * 3,
+        scratch_shapes=[VMEM(w.shape, BF16) for w in weights[:2]] + [pltpu.SemaphoreType.DMA((3,))],
+        compiler_params=grant(8),
+        name="opening",
+    )(*held(arrived.reshape(rows, piece)), *far(*weights))
+
+    fetched = (others[1], others[2])
     results = pl.pallas_call(
         functools.partial(expert_kernel, pieces=pieces),
         out_shape=VMEM((rows, piece), BF16),
-        in_specs=[whole()] * 2 + [anywhere()] * len(fetched),
+        in_specs=[whole()] * 4 + [anywhere()] * len(fetched),
         out_specs=whole(),
         scratch_shapes=[VMEM(w.shape, w.dtype) for w in fetched] + [pltpu.SemaphoreType.DMA((len(fetched),))],
-        compiler_params=grant(16),
+        compiler_params=grant(12),
         name="expert",
-    )(*held(arrived.reshape(rows, piece), others[0]), *far(*fetched))
+    )(*held(inputs, hidden, down, others[0]), *far(*fetched))
     returned = exchange(results.reshape(experts, slots * pieces, piece))
 
     mine = pl.pallas_call(

time: 80.8 us -> 82.7 us (1.024)
  Pallas kernels: 11.2 us -> 12.8 us
    pallas_call x1 -> x2, Pallas kernels: 1.57 us -> 4.72 us  [the longest x1 2.4 us: body(): pl.pallas_call(functools.partial(opening_kernel, pieces=pieces), out_shap...]
    pallas_call x1, Pallas kernels: 5.19 us -> 3.64 us  [body(): pl.pallas_call(functools.partial(expert_kernel, pieces=pieces), out_shape...]
  transfers between devices with their start and end apart: 5 -> 5, of which waited for: 2 -> 2; matrix products, arithmetic and copies ran while one was open for 0% -> 0% of each run, Pallas kernels for 6% -> 10%
where the time goes in v6:
time: 82.7 us; the launch traced here: 82.4 us
  starting transfers between devices  36 us (44%)
  blocking collectives  21.7 us (26%)
  Pallas kernels  12.8 us (15%)
  waiting for transfers between devices  10.1 us (12%)
  local copies, waits for them, and re-layouts  1.61 us (2%)
    all_to_all x1, blocking collectives, body(): arrived = exchange(send.reshape(experts, slots * pieces, piece))  21.7 us
    ppermute x3, starting transfers between devices, body(): others = tuple((lax.ppermute(w, 'tp', swap) for w in weights))  20.9 us
    all_to_all x1, starting transfers between devices, body(): returned = exchange(results.reshape(experts, slots * pieces, piece))  12.1 us
    all_to_all x1, waiting for transfers between devices, body(): returned = exchange(results.reshape(experts, slots * pieces, piece))  8.96 us
    pallas_call x1, Pallas kernels, body(): pl.pallas_call(functools.partial(expert_kernel, pieces=pieces), out_shape...  3.64 us
    pallas_call x1, Pallas kernels, body(): pl.pallas_call(functools.partial(side_kernel, **sizes), out_shape=(VMEM((...  3.42 us
    ppermute x1, starting transfers between devices, body(): other = lax.ppermute(mine, 'tp', swap)  2.98 us
    pallas_call x1, Pallas kernels, body(): pl.pallas_call(functools.partial(opening_kernel, pieces=pieces), out_shap...  2.4 us
  transfers between devices with their start and end apart: 5, of which 2 were waited for; matrix products, arithmetic and copies ran while one was open for 0% of the time, Pallas kernels for 10%

profile of v6, /device:TPU:513, one launch (start us, length us, event | category | flops | bytes accessed | tf_op | source)
XLA Modules:
  0.0 82.4 jit_solution(4244772396583198613)
XLA Ops:
  0.0 20.4 %collective-permute-start = (bf16[2048,384]{1,0:T(8,128)(2,1)}, bf16[2048,384]{1,0:T(8,128)(2,1)S(1)}, u32[]{:S(2)}, u32[]{:S(2)}) collective-permute-start(bf16[2048,384]{1,0:T(8,128)(2,1)} %bitcast.11), channel_id=1, source_target_pairs={{0,1},{1,0},{2,3},{3,2},{4,5},{5,4},{6,7},{7,6},{8,9},{9,8},{10,11... | collective-permute-start | bytes 4718600 | tf_op jit(solution)/shard_map/ppermute | solution.py:302
  20.4 0.0 collective-permute-start.1
  20.4 0.5 collective-permute-start.2
  20.9 2.3 %dispatch.1 = (bf16[512,512]{1,0:T(8,128)(2,1)}, bf16[32,2048]{1,0:T(8,128)(2,1)S(1)}) custom-call(bf16[32,2048]{1,0:T(8,128)(2,1)} %tokens_hbm.1, bf16[2048]{0:T(1024)(128)(2,1)} %gain_hbm.1, s32[6,32]{1,0:T(8,128)} %bitcast.18), custom_call_target="tpu_custom_call" | custom-call | tf_op jit(solution)/shard_map/dispatch/pallas_call | solution.py:304
  23.3 21.7 %all_to_all.10 = bf16[64,8,512]{2,1,0:T(8,128)(2,1)S(1)} all-to-all(bf16[64,8,512]{2,1,0:T(8,128)(2,1)} %bitcast.17), channel_id=1, replica_groups={{126,118,124,116,122,114,120,112,62,54,60,52,58,50,56,48,110,102,108,10..., dimensions={0} | all-to-all | bytes 1048576 | tf_op jit(solution)/shard_map/all_to_all | solution.py:323
  45.0 2.4 %opening.1 = (bf16[128,2048]{1,0:T(8,128)(2,1)S(1)}, bf16[128,384]{1,0:T(8,128)(2,1)S(1)}, bf16[384,2048]{1,0:T(8,128)(2,1)S(1)}) custom-call(bf16[512,512]{1,0:T(8,128)(2,1)S(1)} %bitcast.9, bf16[2048,384]{1,0:T(8,128)(2,1)} %bitcast.12, bf16[2048,384]{1,0:T(8,128)(2,1)} %bitcast.14, bf16[384,2048]{1,0:T(8,128)(2,1)} %bitcast.16), custom_call_target="tpu_custom_call" | custom-call | tf_op jit(solution)/shard_map/opening/pallas_call | solution.py:339
  47.4 0.0 collective-permute-done.gate2_ref
  47.4 0.0 collective-permute-done.1.up2_hbm
  47.4 0.0 copy-start.1
  47.4 0.0 collective-permute-done.2.down2_hbm
  47.4 0.0 copy-start.2
  47.5 1.1 %copy-done.1 = bf16[2048,384]{1,0:T(8,128)(2,1)} copy-done((bf16[2048,384]{1,0:T(8,128)(2,1)}, bf16[2048,384]{1,0:T(8,128)(2,1)S(1)}, u32[]{:S(2)}) %copy-start.1) | copy-done | bytes 1572888
  48.6 0.5 copy-done.2
  49.0 3.6 %expert.1 = bf16[512,512]{1,0:T(8,128)(2,1)} custom-call(bf16[128,2048]{1,0:T(8,128)(2,1)S(1)} %get-tuple-element.15.inputs_ref, bf16[128,384]{1,0:T(8,128)(2,1)S(1)} %get-tuple-element.16.hidden_ref, bf16[384,2048]{1,0:T(8,128)(2,1)S(1)} %get-tuple-element.17.down_ref, bf16[2048,384]{1,0:T(8,128)(2,1)S(1)} %collective-permute-done.gate2_ref, ...), custom_call_target="tpu_custom_call" | custom-call | tf_op jit(solution)/shard_map/expert/pallas_call | solution.py:354
  52.7 12.1 %all-to-all-start.1 = ((bf16[64,8,512]{2,1,0:T(8,128)(2,1)}), bf16[64,8,512]{2,1,0:T(8,128)(2,1)S(1)}, u32[]{:S(2)}, u32[]{:S(2)}) async-start(bf16[64,8,512]{2,1,0:T(8,128)(2,1)} %bitcast.7), calls=%async_computation.1 | async-start | bytes 1048576 | tf_op jit(solution)/shard_map/all_to_all | solution.py:363
  64.8 0.0 copy-start
  64.8 3.4 %side.1 = (f32[128,512]{1,0:T(8,128)S(1)}, bf16[256,512]{1,0:T(8,128)(2,1)S(1)}) custom-call(bf16[32,2048]{1,0:T(8,128)(2,1)S(1)} %get-tuple-element.12.normed_ref, bf16[2048,384]{1,0:T(8,128)(2,1)} %shared_gate_hbm.1, bf16[2048,384]{1,0:T(8,128)(2,1)} %shared_up_hbm.1, bf16[384,2048]{1,0:T(8,128)(2,1)} %shared_down_hbm.1, s32[6,32]{1,0:T(8,128)} %bitcast.19, ...), custom_call_target="tpu_custom_call" | custom-call | tf_op jit(solution)/shard_map/side/pallas_call | solution.py:326
  68.2 9.0 %all-to-all-done.1 = bf16[64,8,512]{2,1,0:T(8,128)(2,1)S(1)} async-done(((bf16[64,8,512]{2,1,0:T(8,128)(2,1)}), bf16[64,8,512]{2,1,0:T(8,128)(2,1)S(1)}, u32[]{:S(2)}, u32[]{:S(2)}) %all-to-all-start.1) | async-done | bytes 524320 | tf_op jit(solution)/shard_map/all_to_all | solution.py:363
  77.2 0.3 combine.1.mine_ref
  77.5 3.0 %collective-permute-start.3 = (f32[128,512]{1,0:T(8,128)S(1)}, f32[128,512]{1,0:T(8,128)S(1)}, u32[]{:S(2)}, u32[]{:S(2)}) collective-permute-start(f32[128,512]{1,0:T(8,128)S(1)} %combine.1.mine_ref), channel_id=1, source_target_pairs={{0,1},{1,0},{2,3},{3,2},{4,5},{5,4},{6,7},{7,6},{8,9},{9,8},{10,11... | collective-permute-start | bytes 786440 | tf_op jit(solution)/shard_map/ppermute | solution.py:373
  80.5 1.2 %collective-permute-done.3.other_ref = f32[128,512]{1,0:T(8,128)S(1)} collective-permute-done((f32[128,512]{1,0:T(8,128)S(1)}, f32[128,512]{1,0:T(8,128)S(1)}, u32[]{:S(2)}, u32[]{:S(2)}) %collective-permute-start.3) | collective-permute-done | bytes 262176 | tf_op jit(solution)/shard_map/ppermute | solution.py:373
  81.6 0.0 copy-done
  81.6 0.8 closing.1
Async XLA Ops:
  0.0 47.4 %collective-permute-start = (bf16[2048,384]{1,0:T(8,128)(2,1)}, bf16[2048,384]{1,0:T(8,128)(2,1)S(1)}, u32[]{:S(2)}, u32[]{:S(2)}) collective-permute-start(bf16[2048,384]{1,0:T(8,128)(2,1)} %bitcast.11), channel_id=1, source_target_pairs={{0,1},{1,0},{2,3},{3,2},{4,5},{5,4},{6,7},{7,6},{8,9},{9,8},{10,11... | collective-permute-start | bytes 4718600 | tf_op jit(solution)/shard_map/ppermute | solution.py:302
  20.4 27.0 %collective-permute-start.1 = (bf16[2048,384]{1,0:T(8,128)(2,1)}, bf16[2048,384]{1,0:T(8,128)(2,1)S(1)}, u32[]{:S(2)}, u32[]{:S(2)}) collective-permute-start(bf16[2048,384]{1,0:T(8,128)(2,1)} %bitcast.13), channel_id=1, source_target_pairs={{0,1},{1,0},{2,3},{3,2},{4,5},{5,4},{6,7},{7,6},{8,9},{9,8},{10,11... | collective-permute-start | bytes 4718600 | tf_op jit(solution)/shard_map/ppermute | solution.py:302
  20.4 27.0 %collective-permute-start.2 = (bf16[384,2048]{1,0:T(8,128)(2,1)}, bf16[384,2048]{1,0:T(8,128)(2,1)S(1)}, u32[]{:S(2)}, u32[]{:S(2)}) collective-permute-start(bf16[384,2048]{1,0:T(8,128)(2,1)} %bitcast.15), channel_id=1, source_target_pairs={{0,1},{1,0},{2,3},{3,2},{4,5},{5,4},{6,7},{7,6},{8,9},{9,8},{10,11... | collective-permute-start | bytes 4718600 | tf_op jit(solution)/shard_map/ppermute | solution.py:302
  47.4 1.2 %copy-start.1 = (bf16[2048,384]{1,0:T(8,128)(2,1)}, bf16[2048,384]{1,0:T(8,128)(2,1)S(1)}, u32[]{:S(2)}) copy-start(bf16[2048,384]{1,0:T(8,128)(2,1)S(1)} %collective-permute-done.1.up2_hbm) | copy-start | bytes 4718596
  47.4 1.6 %copy-start.2 = (bf16[384,2048]{1,0:T(8,128)(2,1)}, bf16[384,2048]{1,0:T(8,128)(2,1)S(1)}, u32[]{:S(2)}) copy-start(bf16[384,2048]{1,0:T(8,128)(2,1)S(1)} %collective-permute-done.2.down2_hbm) | copy-start | bytes 4718596
  52.7 24.5 %all-to-all-start.1 = ((bf16[64,8,512]{2,1,0:T(8,128)(2,1)}), bf16[64,8,512]{2,1,0:T(8,128)(2,1)S(1)}, u32[]{:S(2)}, u32[]{:S(2)}) async-start(bf16[64,8,512]{2,1,0:T(8,128)(2,1)} %bitcast.7), calls=%async_computation.1 | async-start | bytes 1048576 | tf_op jit(solution)/shard_map/all_to_all | solution.py:363
  64.8 16.8 %copy-start = (bf16[1024]{0:T(1024)(128)(2,1)S(1)}, bf16[1024]{0:T(1024)(128)(2,1)}, u32[]{:S(2)}) copy-start(bf16[1024]{0:T(1024)(128)(2,1)} %gain_ref.1) | copy-start | bytes 6148
  77.5 4.1 %collective-permute-start.3 = (f32[128,512]{1,0:T(8,128)S(1)}, f32[128,512]{1,0:T(8,128)S(1)}, u32[]{:S(2)}, u32[]{:S(2)}) collective-permute-start(f32[128,512]{1,0:T(8,128)S(1)} %combine.1.mine_ref), channel_id=1, source_target_pairs={{0,1},{1,0},{2,3},{3,2},{4,5},{5,4},{6,7},{7,6},{8,9},{9,8},{10,11... | collective-permute-start | bytes 786440 | tf_op jit(solution)/shard_map/ppermute | solution.py:373

commit v7 on v6

--- a/solution.py
+++ b/solution.py
@@ -99,10 +99,9 @@
     ]
     for load in loads:
         load.start()
-    loads[0].wait()
+    for load in loads:
+        load.wait()
     pick = chosen(route_ref[...], core, slots, pieces, experts).astype(BF16)
-    loads[1].wait()
-    loads[2].wait()
     values = tokens_ref[...].astype(F32)
     scaled = values * lax.rsqrt(jnp.mean(values * values, axis=-1, keepdims=True) + EPSILON)
     normed = (scaled * gain_ref[...].astype(F32)[None, :]).astype(BF16)
@@ -127,12 +126,6 @@
 def gathering(half, pieces):
     to, frm = iota((half * pieces, half * pieces), 0), iota((half * pieces, half * pieces), 1)
     return jnp.where(frm == (to % half) * pieces + to // half, 1.0, 0.0).astype(BF16)
-
-
-def swiglu(values, g, u):
-    gate = jnp.dot(values, g[...], preferred_element_type=F32)
-    upward = jnp.dot(values, u[...], preferred_element_type=F32)
-    return (gate * jax.nn.sigmoid(gate) * upward).astype(BF16)
 
 
 def side_kernel(
@@ -172,11 +165,14 @@
     high = mix.astype(BF16)
     mix_ref[: mix.shape[0], :] = high
     mix_ref[mix.shape[0] :, :] = (mix - high.astype(F32)).astype(BF16)
-    for load in loads[2:]:
-        load.wait()
     normed = normed_ref[...]
     tokens, piece = normed.shape[0], normed.shape[1] // pieces
-    hidden = swiglu(normed, shared_gate_ref, shared_up_ref)
+    loads[2].wait()
+    gate = jnp.dot(normed, shared_gate_ref[...], preferred_element_type=F32)
+    loads[3].wait()
+    upward = jnp.dot(normed, shared_up_ref[...], preferred_element_type=F32)
+    hidden = (gate * jax.nn.sigmoid(gate) * upward).astype(BF16)
+    loads[4].wait()
     for q in range(pieces):
         part_ref[q * tokens : (q + 1) * tokens, :] = jnp.dot(
             hidden, shared_down_ref[:, q * piece : (q + 1) * piece], preferred_element_type=F32
@@ -207,40 +203,33 @@
     loads[2].wait()
 
 
-def expert_kernel(
-    inputs_ref,
-    hidden_ref,
-    down_ref,
-    gate2_ref,
-    up2_hbm,
-    down2_hbm,
-    out_ref,
-    up2_ref,
-    down2_ref,
-    sems,
-    *,
-    pieces,
+def middle_kernel(
+    inputs_ref, hidden_ref, down_ref, gate2_hbm, up2_hbm, hidden2_ref, first_ref, gate2_ref, up2_ref, sems
 ):
-    pairs = ((up2_hbm, up2_ref), (down2_hbm, down2_ref))
+    pairs = ((gate2_hbm, gate2_ref), (up2_hbm, up2_ref))
     loads = [pltpu.make_async_copy(src, dst, sems.at[i]) for i, (src, dst) in enumerate(pairs)]
     for load in loads:
         load.start()
+    first_ref[...] = jnp.dot(hidden_ref[...], down_ref[...], preferred_element_type=F32)
+    inputs = inputs_ref[...]
+    loads[0].wait()
+    gate = jnp.dot(inputs, gate2_ref[...], preferred_element_type=F32)
+    loads[1].wait()
+    upward = jnp.dot(inputs, up2_ref[...], preferred_element_type=F32)
+    hidden2_ref[...] = (gate * jax.nn.sigmoid(gate) * upward).astype(BF16)
+
+
+def expert_kernel(hidden2_ref, first_ref, down2_ref, out_ref, *, pieces):
     total, piece = out_ref.shape
     block, half = total // 2, total // pieces // 2
-    inputs = inputs_ref[...]
-    gate = jnp.dot(inputs, gate2_ref[...], preferred_element_type=F32)
-    firsts = jnp.dot(hidden_ref[...], down_ref[...], preferred_element_type=F32)
     back = gathering(half, pieces).T
-    loads[0].wait()
-    upward = jnp.dot(inputs, up2_ref[...], preferred_element_type=F32)
-    hidden2 = (gate * jax.nn.sigmoid(gate) * upward).astype(BF16)
-    loads[1].wait()
+    hidden2 = hidden2_ref[...]
     results = []
     for q in range(pieces):
         span = slice(q * piece, (q + 1) * piece)
         results.append(
             (
-                firsts[:, span] + jnp.dot(hidden2, down2_ref[:, span], preferred_element_type=F32)
+                first_ref[:, span] + jnp.dot(hidden2, down2_ref[:, span], preferred_element_type=F32)
             ).astype(BF16)
         )
     for h in range(2):
@@ -299,7 +288,8 @@
     )
     swap = [(i, (i + 1) % cores) for i in range(cores)]
     weights = (gate_weight[0], up_weight[0], down_weight[0])
-    others = tuple(lax.ppermute(w, "tp", swap) for w in weights)
+    others = tuple(lax.ppermute(w, "tp", swap) for w in weights[:2])
+    others += (lax.ppermute(weights[2], "tp", swap),)
 
     send, normed = pl.pallas_call(
         functools.partial(dispatch_kernel, **sizes),
@@ -350,16 +340,24 @@
         name="opening",
     )(*held(arrived.reshape(rows, piece)), *far(*weights))
 
-    fetched = (others[1], others[2])
+    hidden2, first = pl.pallas_call(
+        middle_kernel,
+        out_shape=(VMEM(hidden.shape, BF16), VMEM(inputs.shape, F32)),
+        in_specs=[whole()] * 3 + [anywhere()] * 2,
+        out_specs=(whole(), whole()),
+        scratch_shapes=[VMEM(w.shape, BF16) for w in others[:2]] + [pltpu.SemaphoreType.DMA((2,))],
+        compiler_params=grant(8),
+        name="middle",
+    )(*held(inputs, hidden, down), *far(*others[:2]))
+
     results = pl.pallas_call(
         functools.partial(expert_kernel, pieces=pieces),
         out_shape=VMEM((rows, piece), BF16),
-        in_specs=[whole()] * 4 + [anywhere()] * len(fetched),
+        in_specs=[whole()] * 3,
         out_specs=whole(),
-        scratch_shapes=[VMEM(w.shape, w.dtype) for w in fetched] + [pltpu.SemaphoreType.DMA((len(fetched),))],
-        compiler_params=grant(12),
+        compiler_params=grant(8),
         name="expert",
-    )(*held(inputs, hidden, down, others[0]), *far(*fetched))
+    )(*held(hidden2, first, others[2]))
     returned = exchange(results.reshape(experts, slots * pieces, piece))
 
     mine = pl.pallas_call(

time: 82.7 us -> 82.9 us (level)
    pallas_call x0 -> x1, Pallas kernels: none -> 2.34 us  [body(): pl.pallas_call(middle_kernel, out_shape=(VMEM(hidden.shape, BF16), VMEM(i...]
    pallas_call x1, Pallas kernels: 3.64 us -> 1.52 us  [body(): pl.pallas_call(functools.partial(expert_kernel, pieces=pieces), out_shape...]
  transfers between devices with their start and end apart: 5 -> 5, of which waited for: 2 -> 2; matrix products, arithmetic and copies ran while one was open for 0% -> 0% of each run, Pallas kernels for 10% -> 12%
where the time goes in v7:
time: 82.9 us; the launch traced here: 82.6 us
  starting transfers between devices  35.9 us (43%)
  blocking collectives  21.7 us (26%)
  Pallas kernels  12.5 us (15%)
  waiting for transfers between devices  10.7 us (13%)
  local copies, waits for them, and re-layouts  1.6 us (2%)
    all_to_all x1, blocking collectives, body(): arrived = exchange(send.reshape(experts, slots * pieces, piece))  21.7 us
    ppermute x2, starting transfers between devices, body(): others = tuple((lax.ppermute(w, 'tp', swap) for w in weights[:2]))  20.4 us
    all_to_all x1, starting transfers between devices, body(): returned = exchange(results.reshape(experts, slots * pieces, piece))  12 us
    all_to_all x1, waiting for transfers between devices, body(): returned = exchange(results.reshape(experts, slots * pieces, piece))  9.54 us
    ppermute x1, starting transfers between devices, body(): other = lax.ppermute(mine, 'tp', swap)  2.98 us
    pallas_call x1, Pallas kernels, body(): pl.pallas_call(functools.partial(side_kernel, **sizes), out_shape=(VMEM((...  2.84 us
    pallas_call x1, Pallas kernels, body(): pl.pallas_call(functools.partial(opening_kernel, pieces=pieces), out_shap...  2.4 us
    pallas_call x1, Pallas kernels, body(): pl.pallas_call(functools.partial(dispatch_kernel, **sizes), out_shape=(pl...  2.37 us
  transfers between devices with their start and end apart: 5, of which 2 were waited for; matrix products, arithmetic and copies ran while one was open for 0% of the time, Pallas kernels for 12%

profile of v7, /device:TPU:513, one launch (start us, length us, event | category | flops | bytes accessed | tf_op | source)
XLA Modules:
  0.0 82.6 jit_solution(15496158074160710841)
XLA Ops:
  0.0 20.4 %collective-permute-start = (bf16[2048,384]{1,0:T(8,128)(2,1)}, bf16[2048,384]{1,0:T(8,128)(2,1)S(1)}, u32[]{:S(2)}, u32[]{:S(2)}) collective-permute-start(bf16[2048,384]{1,0:T(8,128)(2,1)} %bitcast.11), channel_id=1, source_target_pairs={{0,1},{1,0},{2,3},{3,2},{4,5},{5,4},{6,7},{7,6},{8,9},{9,8},{10,11... | collective-permute-start | bytes 4718600 | tf_op jit(solution)/shard_map/ppermute | solution.py:291
  20.4 0.0 collective-permute-start.1
  20.4 0.5 collective-permute-start.2
  20.9 2.4 %dispatch.1 = (bf16[512,512]{1,0:T(8,128)(2,1)}, bf16[32,2048]{1,0:T(8,128)(2,1)S(1)}) custom-call(bf16[32,2048]{1,0:T(8,128)(2,1)} %tokens_hbm.1, bf16[2048]{0:T(1024)(128)(2,1)} %gain_hbm.1, s32[6,32]{1,0:T(8,128)} %bitcast.18), custom_call_target="tpu_custom_call" | custom-call | tf_op jit(solution)/shard_map/dispatch/pallas_call | solution.py:294
  23.3 21.7 %all_to_all.10 = bf16[64,8,512]{2,1,0:T(8,128)(2,1)S(1)} all-to-all(bf16[64,8,512]{2,1,0:T(8,128)(2,1)} %bitcast.17), channel_id=1, replica_groups={{126,118,124,116,122,114,120,112,62,54,60,52,58,50,56,48,110,102,108,10..., dimensions={0} | all-to-all | bytes 1048576 | tf_op jit(solution)/shard_map/all_to_all | solution.py:313
  45.0 2.4 %opening.1 = (bf16[128,2048]{1,0:T(8,128)(2,1)S(1)}, bf16[128,384]{1,0:T(8,128)(2,1)S(1)}, bf16[384,2048]{1,0:T(8,128)(2,1)S(1)}) custom-call(bf16[512,512]{1,0:T(8,128)(2,1)S(1)} %bitcast.9, bf16[2048,384]{1,0:T(8,128)(2,1)} %bitcast.12, bf16[2048,384]{1,0:T(8,128)(2,1)} %bitcast.14, bf16[384,2048]{1,0:T(8,128)(2,1)} %bitcast.16), custom_call_target="tpu_custom_call" | custom-call | tf_op jit(solution)/shard_map/opening/pallas_call | solution.py:329
  47.4 0.0 collective-permute-done.gate2_hbm
  47.5 0.0 copy-start.1
  47.5 0.0 collective-permute-done.1.up2_hbm
  47.5 0.0 copy-start.2
  47.5 1.1 %copy-done.1 = bf16[2048,384]{1,0:T(8,128)(2,1)} copy-done((bf16[2048,384]{1,0:T(8,128)(2,1)}, bf16[2048,384]{1,0:T(8,128)(2,1)S(1)}, u32[]{:S(2)}) %copy-start.1) | copy-done | bytes 1572888
  48.6 0.5 copy-done.2
  49.1 2.3 %middle.1 = (bf16[128,384]{1,0:T(8,128)(2,1)S(1)}, f32[128,2048]{1,0:T(8,128)S(1)}) custom-call(bf16[128,2048]{1,0:T(8,128)(2,1)S(1)} %get-tuple-element.17.inputs_ref, bf16[128,384]{1,0:T(8,128)(2,1)S(1)} %get-tuple-element.18.hidden_ref, bf16[384,2048]{1,0:T(8,128)(2,1)S(1)} %get-tuple-element.19.down_ref, bf16[2048,384]{1,0:T(8,128)(2,1)} %copy-done.1, ...), custom_call_target="tpu_custom_call" | custom-call | tf_op jit(solution)/shard_map/middle/pallas_call | solution.py:343
  51.4 0.0 collective-permute-done.2.down2_ref
  51.4 1.5 %expert.1 = bf16[512,512]{1,0:T(8,128)(2,1)} custom-call(bf16[128,384]{1,0:T(8,128)(2,1)S(1)} %get-tuple-element.20.hidden2_ref, f32[128,2048]{1,0:T(8,128)S(1)} %get-tuple-element.21.first_ref, bf16[384,2048]{1,0:T(8,128)(2,1)S(1)} %collective-permute-done.2.down2_ref), custom_call_target="tpu_custom_call" | custom-call | tf_op jit(solution)/shard_map/expert/pallas_call | solution.py:353
  53.0 12.0 %all-to-all-start.1 = ((bf16[64,8,512]{2,1,0:T(8,128)(2,1)}), bf16[64,8,512]{2,1,0:T(8,128)(2,1)S(1)}, u32[]{:S(2)}, u32[]{:S(2)}) async-start(bf16[64,8,512]{2,1,0:T(8,128)(2,1)} %bitcast.7), calls=%async_computation.1 | async-start | bytes 1048576 | tf_op jit(solution)/shard_map/all_to_all | solution.py:361
  65.0 0.0 copy-start
  65.0 2.8 %side.1 = (f32[128,512]{1,0:T(8,128)S(1)}, bf16[256,512]{1,0:T(8,128)(2,1)S(1)}) custom-call(bf16[32,2048]{1,0:T(8,128)(2,1)S(1)} %get-tuple-element.14.normed_ref, bf16[2048,384]{1,0:T(8,128)(2,1)} %shared_gate_hbm.1, bf16[2048,384]{1,0:T(8,128)(2,1)} %shared_up_hbm.1, bf16[384,2048]{1,0:T(8,128)(2,1)} %shared_down_hbm.1, s32[6,32]{1,0:T(8,128)} %bitcast.19, ...), custom_call_target="tpu_custom_call" | custom-call | tf_op jit(solution)/shard_map/side/pallas_call | solution.py:316
  67.9 9.5 %all-to-all-done.1 = bf16[64,8,512]{2,1,0:T(8,128)(2,1)S(1)} async-done(((bf16[64,8,512]{2,1,0:T(8,128)(2,1)}), bf16[64,8,512]{2,1,0:T(8,128)(2,1)S(1)}, u32[]{:S(2)}, u32[]{:S(2)}) %all-to-all-start.1) | async-done | bytes 524320 | tf_op jit(solution)/shard_map/all_to_all | solution.py:361
  77.4 0.3 combine.1.mine_ref
  77.7 3.0 %collective-permute-start.3 = (f32[128,512]{1,0:T(8,128)S(1)}, f32[128,512]{1,0:T(8,128)S(1)}, u32[]{:S(2)}, u32[]{:S(2)}) collective-permute-start(f32[128,512]{1,0:T(8,128)S(1)} %combine.1.mine_ref), channel_id=1, source_target_pairs={{0,1},{1,0},{2,3},{3,2},{4,5},{5,4},{6,7},{7,6},{8,9},{9,8},{10,11... | collective-permute-start | bytes 786440 | tf_op jit(solution)/shard_map/ppermute | solution.py:371
  80.7 1.2 %collective-permute-done.3.other_ref = f32[128,512]{1,0:T(8,128)S(1)} collective-permute-done((f32[128,512]{1,0:T(8,128)S(1)}, f32[128,512]{1,0:T(8,128)S(1)}, u32[]{:S(2)}, u32[]{:S(2)}) %collective-permute-start.3) | collective-permute-done | bytes 262176 | tf_op jit(solution)/shard_map/ppermute | solution.py:371
  81.9 0.0 copy-done
  81.9 0.8 closing.1
Async XLA Ops:
  0.0 47.4 %collective-permute-start = (bf16[2048,384]{1,0:T(8,128)(2,1)}, bf16[2048,384]{1,0:T(8,128)(2,1)S(1)}, u32[]{:S(2)}, u32[]{:S(2)}) collective-permute-start(bf16[2048,384]{1,0:T(8,128)(2,1)} %bitcast.11), channel_id=1, source_target_pairs={{0,1},{1,0},{2,3},{3,2},{4,5},{5,4},{6,7},{7,6},{8,9},{9,8},{10,11... | collective-permute-start | bytes 4718600 | tf_op jit(solution)/shard_map/ppermute | solution.py:291
  20.4 27.1 %collective-permute-start.1 = (bf16[2048,384]{1,0:T(8,128)(2,1)}, bf16[2048,384]{1,0:T(8,128)(2,1)S(1)}, u32[]{:S(2)}, u32[]{:S(2)}) collective-permute-start(bf16[2048,384]{1,0:T(8,128)(2,1)} %bitcast.13), channel_id=1, source_target_pairs={{0,1},{1,0},{2,3},{3,2},{4,5},{5,4},{6,7},{7,6},{8,9},{9,8},{10,11... | collective-permute-start | bytes 4718600 | tf_op jit(solution)/shard_map/ppermute | solution.py:291
  20.4 31.0 %collective-permute-start.2 = (bf16[384,2048]{1,0:T(8,128)(2,1)}, bf16[384,2048]{1,0:T(8,128)(2,1)S(1)}, u32[]{:S(2)}, u32[]{:S(2)}) collective-permute-start(bf16[384,2048]{1,0:T(8,128)(2,1)} %bitcast.15), channel_id=1, source_target_pairs={{0,1},{1,0},{2,3},{3,2},{4,5},{5,4},{6,7},{7,6},{8,9},{9,8},{10,11... | collective-permute-start | bytes 4718600 | tf_op jit(solution)/shard_map/ppermute | solution.py:292
  47.5 1.2 %copy-start.1 = (bf16[2048,384]{1,0:T(8,128)(2,1)}, bf16[2048,384]{1,0:T(8,128)(2,1)S(1)}, u32[]{:S(2)}) copy-start(bf16[2048,384]{1,0:T(8,128)(2,1)S(1)} %collective-permute-done.gate2_hbm) | copy-start | bytes 4718596
  47.5 1.6 %copy-start.2 = (bf16[2048,384]{1,0:T(8,128)(2,1)}, bf16[2048,384]{1,0:T(8,128)(2,1)S(1)}, u32[]{:S(2)}) copy-start(bf16[2048,384]{1,0:T(8,128)(2,1)S(1)} %collective-permute-done.1.up2_hbm) | copy-start | bytes 4718596
  53.0 24.5 %all-to-all-start.1 = ((bf16[64,8,512]{2,1,0:T(8,128)(2,1)}), bf16[64,8,512]{2,1,0:T(8,128)(2,1)S(1)}, u32[]{:S(2)}, u32[]{:S(2)}) async-start(bf16[64,8,512]{2,1,0:T(8,128)(2,1)} %bitcast.7), calls=%async_computation.1 | async-start | bytes 1048576 | tf_op jit(solution)/shard_map/all_to_all | solution.py:361
  65.0 16.8 %copy-start = (bf16[1024]{0:T(1024)(128)(2,1)S(1)}, bf16[1024]{0:T(1024)(128)(2,1)}, u32[]{:S(2)}) copy-start(bf16[1024]{0:T(1024)(128)(2,1)} %gain_ref.1) | copy-start | bytes 6148
  77.7 4.1 %collective-permute-start.3 = (f32[128,512]{1,0:T(8,128)S(1)}, f32[128,512]{1,0:T(8,128)S(1)}, u32[]{:S(2)}, u32[]{:S(2)}) collective-permute-start(f32[128,512]{1,0:T(8,128)S(1)} %combine.1.mine_ref), channel_id=1, source_target_pairs={{0,1},{1,0},{2,3},{3,2},{4,5},{5,4},{6,7},{7,6},{8,9},{9,8},{10,11... | collective-permute-start | bytes 786440 | tf_op jit(solution)/shard_map/ppermute | solution.py:371

commit v8 on v7

--- a/solution.py
+++ b/solution.py
@@ -47,7 +47,7 @@
     def spread(i):
         return i // 2 + i % 2 * (side // 2)
 
-    return experts - 1 - spread(block // side) * side - spread(block % side)
+    return experts - 1 - spread(block % side) * side - block // side
 
 
 def chosen(route, core, slots, pieces, experts, values=None):
@@ -135,8 +135,10 @@
     shared_down_hbm,
     route_hbm,
     weight_hbm,
+    kept_hbm,
     part_ref,
     mix_ref,
+    kept_ref,
     shared_gate_ref,
     shared_up_ref,
     shared_down_ref,
@@ -155,6 +157,7 @@
         (shared_gate_hbm, shared_gate_ref),
         (shared_up_hbm, shared_up_ref),
         (shared_down_hbm, shared_down_ref),
+        (kept_hbm.at[pl.ds(0, kept_ref.shape[0])], kept_ref),
     )
     loads = [pltpu.make_async_copy(src, dst, sems.at[i]) for i, (src, dst) in enumerate(pairs)]
     for load in loads:
@@ -177,12 +180,26 @@
         part_ref[q * tokens : (q + 1) * tokens, :] = jnp.dot(
             hidden, shared_down_ref[:, q * piece : (q + 1) * piece], preferred_element_type=F32
         )
+    loads[5].wait()
 
 
 def opening_kernel(
-    rows_ref, gate_hbm, up_hbm, down_hbm, inputs_ref, hidden_ref, down_ref, gate_ref, up_ref, sems, *, pieces
+    rows_ref,
+    kept_ref,
+    gate_hbm,
+    up_hbm,
+    down_hbm,
+    inputs_ref,
+    hidden_ref,
+    down_ref,
+    gate_ref,
+    up_ref,
+    sems,
+    *,
+    pieces,
 ):
-    pairs = ((gate_hbm, gate_ref), (up_hbm, up_ref), (down_hbm, down_ref))
+    kept, rest = kept_ref.shape[0], gate_ref.shape[0]
+    pairs = ((gate_hbm.at[pl.ds(kept, rest)], gate_ref), (up_hbm, up_ref), (down_hbm, down_ref))
     loads = [pltpu.make_async_copy(src, dst, sems.at[i]) for i, (src, dst) in enumerate(pairs)]
     for load in loads:
         load.start()
@@ -195,8 +212,9 @@
         for q in range(pieces):
             inputs_ref[h * half : (h + 1) * half, q * piece : (q + 1) * piece] = part[q * half : (q + 1) * half]
     inputs = inputs_ref[...]
+    gate = jnp.dot(inputs[:, :kept], kept_ref[...], preferred_element_type=F32)
     loads[0].wait()
-    gate = jnp.dot(inputs, gate_ref[...], preferred_element_type=F32)
+    gate += jnp.dot(inputs[:, kept:], gate_ref[...], preferred_element_type=F32)
     loads[1].wait()
     upward = jnp.dot(inputs, up_ref[...], preferred_element_type=F32)
     hidden_ref[...] = (gate * jax.nn.sigmoid(gate) * upward).astype(BF16)
@@ -313,18 +331,19 @@
     arrived = exchange(send.reshape(experts, slots * pieces, piece))
 
     loaded = (shared_gate, shared_up, shared_down, route_expert.T, route_weight.T)
-    part, mix = pl.pallas_call(
+    part, mix, kept = pl.pallas_call(
         functools.partial(side_kernel, **sizes),
         out_shape=(
             VMEM((pieces * local_tokens, piece), F32),
             VMEM((2 * pieces * local_tokens, rows), BF16),
+            VMEM((weights[0].shape[0] // 2, weights[0].shape[1]), BF16),
         ),
-        in_specs=[whole()] + [anywhere()] * len(loaded),
-        out_specs=(whole(), whole()),
-        scratch_shapes=[VMEM(w.shape, w.dtype) for w in loaded] + [pltpu.SemaphoreType.DMA((len(loaded),))],
+        in_specs=[whole()] + [anywhere()] * 6,
+        out_specs=(whole(),) * 3,
+        scratch_shapes=[VMEM(w.shape, w.dtype) for w in loaded] + [pltpu.SemaphoreType.DMA((6,))],
         compiler_params=grant(12),
         name="side",
-    )(*held(normed), *far(*loaded))
+    )(*held(normed), *far(*loaded, weights[0]))
 
     inputs, hidden, down = pl.pallas_call(
         functools.partial(opening_kernel, pieces=pieces),
@@ -333,12 +352,12 @@
             VMEM((rows // pieces, weights[0].shape[1]), BF16),
             VMEM(weights[2].shape, BF16),
         ),
-        in_specs=[whole()] + [anywhere()] * 3,
+        in_specs=[whole()] * 2 + [anywhere()] * 3,
         out_specs=(whole(),) * 3,
-        scratch_shapes=[VMEM(w.shape, BF16) for w in weights[:2]] + [pltpu.SemaphoreType.DMA((3,))],
+        scratch_shapes=[VMEM(kept.shape, BF16), VMEM(weights[1].shape, BF16), pltpu.SemaphoreType.DMA((3,))],
         compiler_params=grant(8),
         name="opening",
-    )(*held(arrived.reshape(rows, piece)), *far(*weights))
+    )(*held(arrived.reshape(rows, piece), kept), *far(*weights))
 
     hidden2, first = pl.pallas_call(
         middle_kernel,

time: 82.9 us -> 80.3 us (0.969)
  starting transfers between devices: 35.9 us -> 33.5 us
  local copies, waits for them, and re-layouts: 1.6 us -> 0.01 us
  waiting for transfers between devices: 10.7 us -> 12.2 us
  Pallas kernels: 12.5 us -> 11.5 us
  blocking collectives: 21.7 us -> 22.7 us
    all_to_all x1, starting transfers between devices: 12 us -> 8.29 us  [body(): arrived = exchange(send.reshape(experts, slots * pieces, piece))]
    unnamed x6 -> x2, local copies, waits for them, and re-layouts: 1.6 us -> 0.01 us
    all_to_all x1, waiting for transfers between devices: 9.54 us -> 11.1 us  [body(): arrived = exchange(send.reshape(experts, slots * pieces, piece))]
    ppermute x1, starting transfers between devices: 2.98 us -> 4.32 us  [body(): other = lax.ppermute(mine, 'tp', swap)]
    all_to_all x1, blocking collectives: 21.7 us -> 22.7 us  [body(): returned = exchange(results.reshape(experts, slots * pieces, piece))]
where the time goes in v8:
time: 80.3 us; the launch traced here: 80 us
  starting transfers between devices  33.5 us (42%)
  blocking collectives  22.7 us (28%)
  waiting for transfers between devices  12.2 us (15%)
  Pallas kernels  11.5 us (14%)
    all_to_all x1, blocking collectives, body(): returned = exchange(results.reshape(experts, slots * pieces, piece))  22.7 us
    ppermute x2, starting transfers between devices, body(): others = tuple((lax.ppermute(w, 'tp', swap) for w in weights[:2]))  20.4 us
    all_to_all x1, waiting for transfers between devices, body(): arrived = exchange(send.reshape(experts, slots * pieces, piece))  11.1 us
    all_to_all x1, starting transfers between devices, body(): arrived = exchange(send.reshape(experts, slots * pieces, piece))  8.29 us
    ppermute x1, starting transfers between devices, body(): other = lax.ppermute(mine, 'tp', swap)  4.32 us
    pallas_call x1, Pallas kernels, body(): pl.pallas_call(functools.partial(side_kernel, **sizes), out_shape=(VMEM((...  2.85 us
    pallas_call x1, Pallas kernels, body(): pl.pallas_call(middle_kernel, out_shape=(VMEM(hidden.shape, BF16), VMEM(i...  2.34 us
    pallas_call x1, Pallas kernels, body(): pl.pallas_call(functools.partial(dispatch_kernel, **sizes), out_shape=(pl...  2.31 us
  transfers between devices with their start and end apart: 5, of which 2 were waited for; matrix products, arithmetic and copies ran while one was open for 0% of the time, Pallas kernels for 12%

profile of v8, /device:TPU:513, one launch (start us, length us, event | category | flops | bytes accessed | tf_op | source)
XLA Modules:
  0.0 80.0 jit_solution(14613462787184887387)
XLA Ops:
  0.0 20.4 %collective-permute-start = (bf16[2048,384]{1,0:T(8,128)(2,1)}, bf16[2048,384]{1,0:T(8,128)(2,1)}, u32[]{:S(2)}, u32[]{:S(2)}) collective-permute-start(bf16[2048,384]{1,0:T(8,128)(2,1)} %bitcast.12), channel_id=1, source_target_pairs={{0,1},{1,0},{2,3},{3,2},{4,5},{5,4},{6,7},{7,6},{8,9},{9,8},{10,11... | collective-permute-start | bytes 4718600 | tf_op jit(solution)/shard_map/ppermute | solution.py:309
  20.4 0.0 collective-permute-start.1
  20.4 0.5 collective-permute-start.2
  20.9 2.3 %dispatch.1 = (bf16[512,512]{1,0:T(8,128)(2,1)}, bf16[32,2048]{1,0:T(8,128)(2,1)S(1)}) custom-call(bf16[32,2048]{1,0:T(8,128)(2,1)} %tokens_hbm.1, bf16[2048]{0:T(1024)(128)(2,1)} %gain_hbm.1, s32[6,32]{1,0:T(8,128)} %bitcast.20), custom_call_target="tpu_custom_call" | custom-call | tf_op jit(solution)/shard_map/dispatch/pallas_call | solution.py:312
  23.2 8.3 %all-to-all-start = ((bf16[64,8,512]{2,1,0:T(8,128)(2,1)}), bf16[64,8,512]{2,1,0:T(8,128)(2,1)S(1)}, u32[]{:S(2)}, u32[]{:S(2)}) async-start(bf16[64,8,512]{2,1,0:T(8,128)(2,1)} %bitcast.19), calls=%async_computation | async-start | bytes 1048576 | tf_op jit(solution)/shard_map/all_to_all | solution.py:331
  31.5 2.8 %side.1 = (f32[128,512]{1,0:T(8,128)S(1)}, bf16[256,512]{1,0:T(8,128)(2,1)S(1)}, bf16[1024,384]{1,0:T(8,128)(2,1)S(1)}) custom-call(bf16[32,2048]{1,0:T(8,128)(2,1)S(1)} %get-tuple-element.15.normed_ref, bf16[2048,384]{1,0:T(8,128)(2,1)} %shared_gate_hbm.1, bf16[2048,384]{1,0:T(8,128)(2,1)} %shared_up_hbm.1, bf16[384,2048]{1,0:T(8,128)(2,1)} %shared_down_hbm.1, ...), custom_call_target="tpu_custom_call" | custom-call | tf_op jit(solution)/shard_map/side/pallas_call | solution.py:334
  34.4 11.1 %all-to-all-done = bf16[64,8,512]{2,1,0:T(8,128)(2,1)S(1)} async-done(((bf16[64,8,512]{2,1,0:T(8,128)(2,1)}), bf16[64,8,512]{2,1,0:T(8,128)(2,1)S(1)}, u32[]{:S(2)}, u32[]{:S(2)}) %all-to-all-start) | async-done | bytes 524320 | tf_op jit(solution)/shard_map/all_to_all | solution.py:331
  45.4 2.2 %opening.1 = (bf16[128,2048]{1,0:T(8,128)(2,1)S(1)}, bf16[128,384]{1,0:T(8,128)(2,1)S(1)}, bf16[384,2048]{1,0:T(8,128)(2,1)S(1)}) custom-call(bf16[512,512]{1,0:T(8,128)(2,1)S(1)} %bitcast.9, bf16[1024,384]{1,0:T(8,128)(2,1)S(1)} %get-tuple-element.18.kept_ref, bf16[2048,384]{1,0:T(8,128)(2,1)} %bitcast.14, bf16[2048,384]{1,0:T(8,128)(2,1)} %bitcast.16, ...), custom_call_target="tpu_custom_call" | custom-call | tf_op jit(solution)/shard_map/opening/pallas_call | solution.py:348
  47.7 0.0 collective-permute-done.gate2_hbm
  47.7 0.0 collective-permute-done.1.up2_hbm
  47.7 2.3 %middle.1 = (bf16[128,384]{1,0:T(8,128)(2,1)S(1)}, f32[128,2048]{1,0:T(8,128)S(1)}) custom-call(bf16[128,2048]{1,0:T(8,128)(2,1)S(1)} %get-tuple-element.19.inputs_ref, bf16[128,384]{1,0:T(8,128)(2,1)S(1)} %get-tuple-element.20.hidden_ref, bf16[384,2048]{1,0:T(8,128)(2,1)S(1)} %get-tuple-element.21.down_ref, ...), custom_call_target="tpu_custom_call" | custom-call | tf_op jit(solution)/shard_map/middle/pallas_call | solution.py:362
  50.0 0.0 collective-permute-done.2.down2_ref
  50.1 0.7 expert.1
  50.8 0.0 copy-start
  50.8 22.7 %all_to_all.10 = bf16[64,8,512]{2,1,0:T(8,128)(2,1)S(1)} all-to-all(bf16[64,8,512]{2,1,0:T(8,128)(2,1)S(1)} %bitcast.10), channel_id=1, replica_groups={{126,62,110,46,94,30,78,14,124,60,108,44,92,28,76,12,122,58,106,42,90,2..., dimensions={0} | all-to-all | bytes 1048576 | tf_op jit(solution)/shard_map/all_to_all | solution.py:380
  73.5 0.3 combine.1.mine_ref
  73.8 4.3 %collective-permute-start.3 = (f32[128,512]{1,0:T(8,128)S(1)}, f32[128,512]{1,0:T(8,128)S(1)}, u32[]{:S(2)}, u32[]{:S(2)}) collective-permute-start(f32[128,512]{1,0:T(8,128)S(1)} %combine.1.mine_ref), channel_id=1, source_target_pairs={{0,1},{1,0},{2,3},{3,2},{4,5},{5,4},{6,7},{7,6},{8,9},{9,8},{10,11... | collective-permute-start | bytes 786440 | tf_op jit(solution)/shard_map/ppermute | solution.py:390
  78.1 1.2 %collective-permute-done.3.other_ref = f32[128,512]{1,0:T(8,128)S(1)} collective-permute-done((f32[128,512]{1,0:T(8,128)S(1)}, f32[128,512]{1,0:T(8,128)S(1)}, u32[]{:S(2)}, u32[]{:S(2)}) %collective-permute-start.3) | collective-permute-done | bytes 262176 | tf_op jit(solution)/shard_map/ppermute | solution.py:390
  79.2 0.0 copy-done
  79.3 0.8 closing.1
Async XLA Ops:
  0.0 47.7 %collective-permute-start = (bf16[2048,384]{1,0:T(8,128)(2,1)}, bf16[2048,384]{1,0:T(8,128)(2,1)}, u32[]{:S(2)}, u32[]{:S(2)}) collective-permute-start(bf16[2048,384]{1,0:T(8,128)(2,1)} %bitcast.12), channel_id=1, source_target_pairs={{0,1},{1,0},{2,3},{3,2},{4,5},{5,4},{6,7},{7,6},{8,9},{9,8},{10,11... | collective-permute-start | bytes 4718600 | tf_op jit(solution)/shard_map/ppermute | solution.py:309
  20.4 27.3 %collective-permute-start.1 = (bf16[2048,384]{1,0:T(8,128)(2,1)}, bf16[2048,384]{1,0:T(8,128)(2,1)}, u32[]{:S(2)}, u32[]{:S(2)}) collective-permute-start(bf16[2048,384]{1,0:T(8,128)(2,1)} %bitcast.15), channel_id=1, source_target_pairs={{0,1},{1,0},{2,3},{3,2},{4,5},{5,4},{6,7},{7,6},{8,9},{9,8},{10,11... | collective-permute-start | bytes 4718600 | tf_op jit(solution)/shard_map/ppermute | solution.py:309
  20.4 29.6 %collective-permute-start.2 = (bf16[384,2048]{1,0:T(8,128)(2,1)}, bf16[384,2048]{1,0:T(8,128)(2,1)S(1)}, u32[]{:S(2)}, u32[]{:S(2)}) collective-permute-start(bf16[384,2048]{1,0:T(8,128)(2,1)} %bitcast.17), channel_id=1, source_target_pairs={{0,1},{1,0},{2,3},{3,2},{4,5},{5,4},{6,7},{7,6},{8,9},{9,8},{10,11... | collective-permute-start | bytes 4718600 | tf_op jit(solution)/shard_map/ppermute | solution.py:310
  23.2 22.2 %all-to-all-start = ((bf16[64,8,512]{2,1,0:T(8,128)(2,1)}), bf16[64,8,512]{2,1,0:T(8,128)(2,1)S(1)}, u32[]{:S(2)}, u32[]{:S(2)}) async-start(bf16[64,8,512]{2,1,0:T(8,128)(2,1)} %bitcast.19), calls=%async_computation | async-start | bytes 1048576 | tf_op jit(solution)/shard_map/all_to_all | solution.py:331
  50.8 28.5 %copy-start = (bf16[1024]{0:T(1024)(128)(2,1)S(1)}, bf16[1024]{0:T(1024)(128)(2,1)}, u32[]{:S(2)}) copy-start(bf16[1024]{0:T(1024)(128)(2,1)} %gain_ref.1) | copy-start | bytes 6148
  73.8 5.5 %collective-permute-start.3 = (f32[128,512]{1,0:T(8,128)S(1)}, f32[128,512]{1,0:T(8,128)S(1)}, u32[]{:S(2)}, u32[]{:S(2)}) collective-permute-start(f32[128,512]{1,0:T(8,128)S(1)} %combine.1.mine_ref), channel_id=1, source_target_pairs={{0,1},{1,0},{2,3},{3,2},{4,5},{5,4},{6,7},{7,6},{8,9},{9,8},{10,11... | collective-permute-start | bytes 786440 | tf_op jit(solution)/shard_map/ppermute | solution.py:390
